TPU v7x, 128 devices: a whole 4x4x4 slice. The times are simulated.
128 devices in a mesh: sp: 16 (over z, y), tp: 8 (over x, core).
Axes of the slice: x: 4, y: 4, z: 4, core: 2. Of those that a mesh axis runs over, the one named last changes fastest.
Arguments:
- values_in: bfloat16 [4, 16384, 1024], P(None, 'sp', 'tp'), may hold values from -6 to 6
- gates_in: bfloat16 [4, 16384, 1024], P(None, 'sp', 'tp'), may hold values from -8 to 8
- conv_taps: bfloat16 [31, 1024], P(None, 'tp'), may hold values from -3 to 3
- conv_bias: bfloat16 [1024], P('tp'), may hold values from -3 to 3
- norm_gain: bfloat16 [1024], P('tp'), may hold values from 0.099609375 to 1.8984375
- out_weight: bfloat16 [1024, 4096], P('tp'), may hold values from -0.1875 to 0.1875
- out_grad: bfloat16 [4, 16384, 4096], P(None, 'sp'), may hold values from -1.5 to 1.5
Outputs:
- values_grad: bfloat16 [4, 16384, 1024], P(None, 'sp', 'tp')
- gates_grad: bfloat16 [4, 16384, 1024], P(None, 'sp', 'tp')
- taps_grad: float32 [31, 1024], P(None, 'tp')
- gain_grad: float32 [1024], P('tp')
- bias_grad: float32 [1024], P('tp')
- weight_grad: float32 [1024, 4096], P(('tp', 'sp'))
All inputs are finite; a program needn't handle non-finite values.
Results may differ from a plain program's by a relative error of at most 0.0048.
Values may be sent and summed in bfloat16 or wider, within the bound.
No kernel may reach another device: no remote copies, remote signals or barrier semaphores. Data moves between devices by JAX's collectives and lax.ppermute only.
A program may use at most 128 MiB of HBM per device.

v0:
```python
import jax
import jax.numpy as jnp
from jax import lax
from jax.sharding import PartitionSpec as P

K = 31


EPS = 1e-05


def passed_along(shard, axis, by):
    devices = lax.axis_size(axis)
    pairs = [(i, i + by) for i in range(devices) if 0 <= i + by < devices]
    return lax.ppermute(shard, axis, pairs)


def sent_to_all(shard, axis):
    devices = lax.axis_size(axis)
    return lax.all_to_all(
        jnp.broadcast_to(shard[None], (devices, *shard.shape)), axis, 0, 0, tiled=True
    )


def of_everyone(shard, axis):
    return sent_to_all(shard, axis).sum(axis=0)


def in_one(arrays, axis):
    ends = [0]
    for a in arrays:
        ends.append(ends[-1] + a.size)
    subtotal = of_everyone(jnp.concatenate([a.ravel() for a in arrays]), axis)
    return tuple((subtotal[b:e].reshape(a.shape) for a, b, e in zip(arrays, ends, ends[1:])))


def in_blocks(shard, dim, devices):
    shape = shard.shape
    pieces = shard.reshape(*shape[:dim], devices, shape[dim] // devices, *shape[dim + 1 :])
    return jnp.moveaxis(pieces, dim, 0)


def sent_and_summed(shard, axis, dim):
    pieces = in_blocks(shard, dim, lax.axis_size(axis))
    arrived = lax.all_to_all(pieces, axis, split_axis=0, concat_axis=0, tiled=True)
    return arrived.astype(jnp.float32).sum(axis=0)


def on_device(values_in, gates_in, conv_taps, conv_bias, norm_gain, out_weight, out_grad):
    seq_count, tok_rows, local_chans = values_in.shape
    reach = K - 1
    total_chans = local_chans * lax.axis_size("tp")
    sig = jax.nn.sigmoid(gates_in.astype(jnp.float32))
    gated = (values_in.astype(jnp.float32) * sig).astype(jnp.bfloat16)
    before = passed_along(gated[:, tok_rows - reach :], "sp", 1)
    padded = jnp.concatenate([before, gated], axis=1).astype(jnp.float32)
    tap_rows = conv_taps.astype(jnp.float32)
    conv = jnp.zeros(gated.shape, jnp.float32) + conv_bias.astype(jnp.float32)
    for tap_index in range(K):
        conv = conv + tap_rows[tap_index] * padded[:, tap_index : tap_index + tok_rows]
    totals = in_one((jnp.sum(conv, axis=-1), jnp.sum(conv * conv, axis=-1)), "tp")
    channel_mean = totals[0][..., None] / total_chans
    variance = totals[1][..., None] / total_chans - channel_mean * channel_mean
    inverse = lax.rsqrt(variance + EPS)
    normed = (conv - channel_mean) * inverse
    gain = norm_gain.astype(jnp.float32)
    scaled = normed * gain
    swished = jax.nn.silu(scaled).astype(jnp.bfloat16)
    flat_swished = swished.reshape(seq_count * tok_rows, local_chans)
    flat_cot = out_grad.reshape(seq_count * tok_rows, out_grad.shape[2])
    weight_grad = sent_and_summed(
        lax.dot_general(
            flat_swished, flat_cot, (((0,), (0,)), ((), ())), preferred_element_type=jnp.float32
        ).astype(jnp.bfloat16),
        "sp",
        0,
    )
    swish_grad = jnp.einsum("std,cd->stc", out_grad, out_weight, preferred_element_type=jnp.float32)
    scaled_sig = jax.nn.sigmoid(scaled)
    scaled_grad = swish_grad * scaled_sig * (1.0 + scaled * (1.0 - scaled_sig))
    gain_local = jnp.sum(scaled_grad * normed, axis=(0, 1))
    normed_grad = scaled_grad * gain
    back_sums = in_one(
        (jnp.sum(normed_grad, axis=-1), jnp.sum(normed_grad * normed, axis=-1)), "tp"
    )
    conv_grad = inverse * (
        normed_grad
        - back_sums[0][..., None] / total_chans
        - normed * (back_sums[1][..., None] / total_chans)
    )
    bias_local = jnp.sum(conv_grad, axis=(0, 1))
    taps_local = jnp.stack(
        [
            jnp.sum(conv_grad * padded[:, tap_index : tap_index + tok_rows], axis=(0, 1))
            for tap_index in range(K)
        ]
    )
    taps_grad, gain_grad, bias_grad = in_one((taps_local, gain_local, bias_local), "sp")
    wide_grad = jnp.pad(conv_grad, ((0, 0), (reach, reach), (0, 0)))
    spread = jnp.zeros((seq_count, tok_rows + reach, local_chans), jnp.float32)
    for tap_index in range(K):
        begin = reach - tap_index
        spread = spread + tap_rows[tap_index] * wide_grad[:, begin : begin + tok_rows + reach]
    arrived = passed_along(spread[:, :reach], "sp", -1)
    own = spread[:, reach:]
    gated_grad = jnp.concatenate(
        [own[:, : tok_rows - reach], own[:, tok_rows - reach :] + arrived], axis=1
    )
    values_grad = (gated_grad * sig).astype(jnp.bfloat16)
    gates_grad = (gated_grad * values_in.astype(jnp.float32) * sig * (1.0 - sig)).astype(
        jnp.bfloat16
    )
    return (values_grad, gates_grad, taps_grad, gain_grad, bias_grad, weight_grad)


def solution(mesh):
    return jax.shard_map(
        on_device,
        mesh=mesh,
        in_specs=(
            P(None, "sp", "tp"),
            P(None, "sp", "tp"),
            P(None, "tp"),
            P("tp"),
            P("tp"),
            P("tp", None),
            P(None, "sp", None),
        ),
        out_specs=(
            P(None, "sp", "tp"),
            P(None, "sp", "tp"),
            P(None, "tp"),
            P("tp"),
            P("tp"),
            P(("tp", "sp"), None),
        ),
        check_vma=False,
    )
```

profile of v0, /device:TPU:0, one launch (start us, length us, event | category | flops | bytes accessed | tf_op | source)
XLA Modules:
  0.0 135.1 jit_solution(6444838489050009195)
XLA Ops:
  0.6 0.0 copy-start
  0.7 2.2 %fusion.2 = bf16[4,1024,128]{2,1,0:T(8,128)(2,1)S(1)} fusion(bf16[4,1024,128]{2,1,0:T(8,128)(2,1)} %param.7, bf16[4,1024,128]{2,1,0:T(8,128)(2,1)} %param.8), kind=kLoop, calls=%fused_computation.6 | loop fusion | flops 3670016 | bytes 3145728 | tf_op jit(solution)/shard_map/convert_element_type | solution.py:54
  2.9 3.6 %collective-permute-start = (bf16[4,30,128]{2,1,0:T(8,128)(2,1)S(1)}, bf16[4,30,128]{2,1,0:T(8,128)(2,1)S(1)}, u32[]{:S(2)}, u32[]{:S(2)}) collective-permute-start(bf16[4,30,128]{2,1,0:T(8,128)(2,1)S(1)} %slice.525), channel_id=1, source_target_pairs={{0,8},{8,16},{16,24},{24,32},{32,40},{40,48},{48,56},{56,64},{64,7... | collective-permute-start | bytes 92168 | tf_op jit(solution)/shard_map/ppermute | solution.py:15
  6.8 1.2 collective-permute-done
  8.0 0.2 maximum_convert_fusion
  8.3 9.6 %fusion.12 = (f32[4,1024]{1,0:T(4,128)S(1)}, f32[4,1024]{1,0:T(4,128)S(1)}, f32[4,1024,128]{2,1,0:T(8,128)}) fusion(f32[4,1054,128]{2,1,0:T(8,128)S(1)} %maximum_convert_fusion, f32[128]{0:T(128)S(1)} %get-tuple-element.54, f32[128]{0:T(128)S(1)} %get-tuple-element.55, f32[128]{0:T(128)S(1)} %get-tuple-element.56, f32[128]{0:T(128)S(1)} %get-tuple-element.57, ...), kind=kLoop, calls=%fused_computation.107 | loop fusion | flops 34070528 | bytes 67158016 | tf_op jit(solution)/shard_map/reduce_sum | solution.py:61
  18.1 0.8 broadcast_in_dim.6
  19.0 4.3 %all-to-all-start = ((f32[8,1,8192]{2,1,0:T(1,128)}), f32[8,1,8192]{2,1,0:T(1,128)S(1)}, u32[]{:S(2)}, u32[]{:S(2)}) async-start(f32[8,1,8192]{2,1,0:T(1,128)} %broadcast_in_dim.6), calls=%async_computation | async-start | bytes 524288 | tf_op jit(solution)/shard_map/all_to_all | solution.py:20
  23.3 7.5 %all-to-all-done = f32[8,1,8192]{2,1,0:T(1,128)S(1)} async-done(((f32[8,1,8192]{2,1,0:T(1,128)}), f32[8,1,8192]{2,1,0:T(1,128)S(1)}, u32[]{:S(2)}, u32[]{:S(2)}) %all-to-all-start) | async-done | bytes 262176 | tf_op jit(solution)/shard_map/all_to_all | solution.py:20
  30.8 0.2 reduce_sum.371
  31.1 17.5 %multiply_reduce_fusion = (f32[128]{0:T(128)}, f32[4,1024]{1,0:T(4,128)S(1)}, f32[4,1024]{1,0:T(4,128)S(1)}, f32[4,1024,128]{2,1,0:T(8,128)}) fusion(f32[4,1024,128]{2,1,0:T(8,128)} %get-tuple-element.44, f32[4,1024]{1,0:T(4,128)S(1)} %div.32, f32[4,1024]{1,0:T(4,128)S(1)} %add_rsqrt_fusion, f32[128]{0:T(128)S(1)} %convert_element_type.45, ...), kind=kOutput, calls=%fused_computation.13 | convolution fusion | flops 4303872000 | bytes 38863872 | tf_op jit(solution)/shard_map/std,cd->stc/dot_general | solution.py:78
  48.6 0.1 broadcast_in_dim.7
  48.7 9.9 %all_to_all.23 = f32[8,1,8192]{2,1,0:T(1,128)S(1)} all-to-all(f32[8,1,8192]{2,1,0:T(1,128)S(1)} %broadcast_in_dim.7), channel_id=1, replica_groups=mesh['sp'=16,'tp'=8] {'tp'}, dimensions={0} | all-to-all | bytes 524288 | tf_op jit(solution)/shard_map/all_to_all | solution.py:20
  58.7 0.2 reduce_sum.374
  58.9 7.9 %multiply_reduce_fusion.1 = (f32[128]{0:T(128)S(1)}, f32[128]{0:T(128)S(1)}, f32[128]{0:T(128)S(1)}, f32[128]{0:T(128)S(1)}, f32[128]{0:T(128)S(1)}, /*index=5*/...) fusion(f32[4,1054,128]{2,1,0:T(8,128)S(1)} %maximum_convert_fus, ...), kind=kLoop, calls=%fused_computation.14 | loop fusion | flops 22542080 | bytes 44115456 | tf_op jit(solution)/shard_map/reduce_sum | solution.py:94
  67.1 3.5 %multiply_reduce_fusion.19 = (f32[128]{0:T(128)S(1)}, f32[128]{0:T(128)S(1)}, f32[128]{0:T(128)S(1)}, f32[128]{0:T(128)S(1)}, f32[128]{0:T(128)S(1)}, /*index=5*...) fusion(f32[4,1024,128]{2,1,0:T(8,128)S(1)} %get-tuple-element.4, ...), kind=kLoop, calls=%fused_computation.32 | loop fusion | flops 14153984 | bytes 29367296 | tf_op jit(solution)/shard_map/reduce_sum | solution.py:94
  70.8 9.0 %multiply_add_fusion = f32[4,1054,128]{2,1,0:T(8,128)} fusion(f32[4,1024,128]{2,1,0:T(8,128)S(1)} %get-tuple-element.43, f32[128]{0:T(128)S(1)} %get-tuple-element.54, f32[128]{0:T(128)S(1)} %get-tuple-element.55, f32[128]{0:T(128)S(1)} %copy-done.4, f32[128]{0:T(128)S(1)} %copy-done.6, f32[128]{0:T(128)S(1)} %copy-done.8, f32[128]{0:T(128)S(1)} %copy-done.10, ...), kind=kLoop, calls=%fused_computation.5 | loop fusion | flops 32918528 | bytes 4271616 | tf_op jit(solution)/shard_map/add | solution.py:103
  79.8 0.1 stack.127
  79.9 0.8 broadcast_in_dim.8
  80.7 8.8 %all-to-all-start.2 = ((f32[16,1,4224]{2,1,0:T(1,128)}), f32[16,1,4224]{2,1,0:T(1,128)S(1)}, u32[]{:S(2)}, u32[]{:S(2)}) async-start(f32[16,1,4224]{2,1,0:T(1,128)} %broadcast_in_dim.8), calls=%async_computation.2 | async-start | bytes 540672 | tf_op jit(solution)/shard_map/all_to_all | solution.py:20
  89.5 1.5 %slice.593 = f32[4,30,128]{2,1,0:T(8,128)} slice(f32[4,1054,128]{2,1,0:T(8,128)} %multiply_add_fusion), slice={[0:4], [0:30], [0:128]} | slice | bytes 122880 | tf_op jit(solution)/shard_map/slice | solution.py:104
  91.0 1.3 collective-permute-start.1
  92.3 14.0 %fusion.1 = bf16[16,8,4096]{2,1,0:T(8,128)(2,1)} fusion(bf16[4,1024,4096]{2,1,0:T(8,128)(2,1)} %param.13, f32[4,1024,128]{2,1,0:T(8,128)S(1)} %copy-done.1, f32[128]{0:T(128)S(1)} %convert_element_type.45, f32[4,1024]{1,0:T(4,128)S(1)} %div.32, f32[4,1024]{1,0:T(4,128)S(1)} %add_rsqrt_fusion), kind=kOutput, calls=%fused_computation.2 | convolution fusion | flops 4299685888 | bytes 36733440 | tf_op jit(solution)/shard_map/dot_general | solution.py:72
  106.3 1.7 %slice.591 = f32[4,994,128]{2,1,0:T(8,128)S(1)} slice(f32[4,1054,128]{2,1,0:T(8,128)} %multiply_add_fusion), slice={[0:4], [30:1024], [0:128]} | slice | bytes 4071424 | tf_op jit(solution)/shard_map/slice | solution.py:107
  108.0 8.7 %all-to-all-start.3 = ((bf16[16,8,4096]{2,1,0:T(8,128)(2,1)}), bf16[16,8,4096]{2,1,0:T(8,128)(2,1)}, u32[]{:S(2)}, u32[]{:S(2)}) async-start(bf16[16,8,4096]{2,1,0:T(8,128)(2,1)} %fusion.1), calls=%async_computation.3 | async-start | bytes 2097152 | tf_op jit(solution)/shard_map/all_to_all | solution.py:45
  116.8 0.9 slice_add_fusion
  117.7 3.8 %fusion.5 = (bf16[4,1024,128]{2,1,0:T(8,128)(2,1)}, bf16[4,1024,128]{2,1,0:T(8,128)(2,1)}) fusion(bf16[4,1024,128]{2,1,0:T(8,128)(2,1)} %param.7, f32[4,30,128]{2,1,0:T(8,128)S(1)} %slice_add_fusion, f32[4,994,128]{2,1,0:T(8,128)S(1)} %slice.591, bf16[4,1024,128]{2,1,0:T(8,128)(2,1)} %param.8), kind=kLoop, calls=%fused_computation.9 | loop fusion | flops 6815744 | bytes 6291456 | tf_op jit(solution)/shard_map/convert_element_type | solution.py:110
  121.5 0.2 reduce_sum.408
  121.7 0.5 fusion.13
  122.2 0.6 slice_bitcast_fusion
  122.8 10.3 %all-to-all-done.3 = bf16[16,8,4096]{2,1,0:T(8,128)(2,1)} async-done(((bf16[16,8,4096]{2,1,0:T(8,128)(2,1)}), bf16[16,8,4096]{2,1,0:T(8,128)(2,1)}, u32[]{:S(2)}, u32[]{:S(2)}) %all-to-all-start.3) | async-done | bytes 1048608 | tf_op jit(solution)/shard_map/all_to_all | solution.py:45
  133.1 2.0 %convert_reduce_fusion = f32[8,4096]{1,0:T(8,128)} fusion(bf16[16,8,4096]{2,1,0:T(8,128)(2,1)} %all-to-all-done.3), kind=kLoop, calls=%fused_computation.11 | loop fusion | flops 1015808 | bytes 1179648 | tf_op jit(solution)/shard_map/reduce_sum | solution.py:46
  (144 shorter events, 0.4 us)
Async XLA Ops:
  0.6 30.4 %copy-start = (bf16[128,4096]{1,0:T(8,128)(2,1)S(1)}, bf16[128,4096]{1,0:T(8,128)(2,1)}, u32[]{:S(2)}) copy-start(bf16[128,4096]{1,0:T(8,128)(2,1)} %param.12) | copy-start | bytes 3145732
  2.9 5.2 %collective-permute-start = (bf16[4,30,128]{2,1,0:T(8,128)(2,1)S(1)}, bf16[4,30,128]{2,1,0:T(8,128)(2,1)S(1)}, u32[]{:S(2)}, u32[]{:S(2)}) collective-permute-start(bf16[4,30,128]{2,1,0:T(8,128)(2,1)S(1)} %slice.525), channel_id=1, source_target_pairs={{0,8},{8,16},{16,24},{24,32},{32,40},{40,48},{48,56},{56,64},{64,7... | collective-permute-start | bytes 92168 | tf_op jit(solution)/shard_map/ppermute | solution.py:15
  6.5 11.3 %copy-start.3 = (f32[128]{0:T(128)}, f32[128]{0:T(128)S(1)}, u32[]{:S(2)}) copy-start(f32[128]{0:T(128)S(1)} %get-tuple-element.56) | copy-start | bytes 1540
  6.5 11.3 %copy-start.5 = (f32[128]{0:T(128)}, f32[128]{0:T(128)S(1)}, u32[]{:S(2)}) copy-start(f32[128]{0:T(128)S(1)} %get-tuple-element.57) | copy-start | bytes 1540
  6.5 11.3 %copy-start.7 = (f32[128]{0:T(128)}, f32[128]{0:T(128)S(1)}, u32[]{:S(2)}) copy-start(f32[128]{0:T(128)S(1)} %get-tuple-element.58) | copy-start | bytes 1540
  6.5 11.3 %copy-start.9 = (f32[128]{0:T(128)}, f32[128]{0:T(128)S(1)}, u32[]{:S(2)}) copy-start(f32[128]{0:T(128)S(1)} %get-tuple-element.59) | copy-start | bytes 1540
  6.6 11.3 %copy-start.11 = (f32[128]{0:T(128)}, f32[128]{0:T(128)S(1)}, u32[]{:S(2)}) copy-start(f32[128]{0:T(128)S(1)} %get-tuple-element.60) | copy-start | bytes 1540
  6.6 11.3 %copy-start.13 = (f32[128]{0:T(128)}, f32[128]{0:T(128)S(1)}, u32[]{:S(2)}) copy-start(f32[128]{0:T(128)S(1)} %get-tuple-element.61) | copy-start | bytes 1540
  6.6 11.3 %copy-start.15 = (f32[128]{0:T(128)}, f32[128]{0:T(128)S(1)}, u32[]{:S(2)}) copy-start(f32[128]{0:T(128)S(1)} %get-tuple-element.62) | copy-start | bytes 1540
  6.6 11.3 %copy-start.17 = (f32[128]{0:T(128)}, f32[128]{0:T(128)S(1)}, u32[]{:S(2)}) copy-start(f32[128]{0:T(128)S(1)} %get-tuple-element.63) | copy-start | bytes 1540
  6.6 11.3 %copy-start.19 = (f32[128]{0:T(128)}, f32[128]{0:T(128)S(1)}, u32[]{:S(2)}) copy-start(f32[128]{0:T(128)S(1)} %get-tuple-element.64) | copy-start | bytes 1540
  6.6 11.3 %copy-start.21 = (f32[128]{0:T(128)}, f32[128]{0:T(128)S(1)}, u32[]{:S(2)}) copy-start(f32[128]{0:T(128)S(1)} %get-tuple-element.65) | copy-start | bytes 1540
  6.6 11.3 %copy-start.23 = (f32[128]{0:T(128)}, f32[128]{0:T(128)S(1)}, u32[]{:S(2)}) copy-start(f32[128]{0:T(128)S(1)} %get-tuple-element.66) | copy-start | bytes 1540
  6.6 11.3 %copy-start.25 = (f32[128]{0:T(128)}, f32[128]{0:T(128)S(1)}, u32[]{:S(2)}) copy-start(f32[128]{0:T(128)S(1)} %get-tuple-element.67) | copy-start | bytes 1540
  6.6 11.3 %copy-start.27 = (f32[128]{0:T(128)}, f32[128]{0:T(128)S(1)}, u32[]{:S(2)}) copy-start(f32[128]{0:T(128)S(1)} %get-tuple-element.68) | copy-start | bytes 1540
  6.7 11.3 %copy-start.29 = (f32[128]{0:T(128)}, f32[128]{0:T(128)S(1)}, u32[]{:S(2)}) copy-start(f32[128]{0:T(128)S(1)} %get-tuple-element.69) | copy-start | bytes 1540
  6.7 11.3 %copy-start.31 = (f32[128]{0:T(128)}, f32[128]{0:T(128)S(1)}, u32[]{:S(2)}) copy-start(f32[128]{0:T(128)S(1)} %get-tuple-element.70) | copy-start | bytes 1540
  6.7 11.3 %copy-start.33 = (f32[128]{0:T(128)}, f32[128]{0:T(128)S(1)}, u32[]{:S(2)}) copy-start(f32[128]{0:T(128)S(1)} %get-tuple-element.71) | copy-start | bytes 1540
  6.7 11.3 %copy-start.35 = (f32[128]{0:T(128)}, f32[128]{0:T(128)S(1)}, u32[]{:S(2)}) copy-start(f32[128]{0:T(128)S(1)} %get-tuple-element.72) | copy-start | bytes 1540
  6.7 11.3 %copy-start.37 = (f32[128]{0:T(128)}, f32[128]{0:T(128)S(1)}, u32[]{:S(2)}) copy-start(f32[128]{0:T(128)S(1)} %get-tuple-element.73) | copy-start | bytes 1540
  6.7 11.3 %copy-start.39 = (f32[128]{0:T(128)}, f32[128]{0:T(128)S(1)}, u32[]{:S(2)}) copy-start(f32[128]{0:T(128)S(1)} %get-tuple-element.74) | copy-start | bytes 1540
  6.7 11.3 %copy-start.41 = (f32[128]{0:T(128)}, f32[128]{0:T(128)S(1)}, u32[]{:S(2)}) copy-start(f32[128]{0:T(128)S(1)} %get-tuple-element.75) | copy-start | bytes 1540
  6.7 11.3 %copy-start.43 = (f32[128]{0:T(128)}, f32[128]{0:T(128)S(1)}, u32[]{:S(2)}) copy-start(f32[128]{0:T(128)S(1)} %get-tuple-element.76) | copy-start | bytes 1540
  6.8 11.3 %copy-start.45 = (f32[128]{0:T(128)}, f32[128]{0:T(128)S(1)}, u32[]{:S(2)}) copy-start(f32[128]{0:T(128)S(1)} %get-tuple-element.77) | copy-start | bytes 1540
  6.8 11.3 %copy-start.47 = (f32[128]{0:T(128)}, f32[128]{0:T(128)S(1)}, u32[]{:S(2)}) copy-start(f32[128]{0:T(128)S(1)} %get-tuple-element.78) | copy-start | bytes 1540
  6.8 11.3 %copy-start.49 = (f32[128]{0:T(128)}, f32[128]{0:T(128)S(1)}, u32[]{:S(2)}) copy-start(f32[128]{0:T(128)S(1)} %get-tuple-element.79) | copy-start | bytes 1540
  8.3 15.0 %copy-start.61 = (bf16[128]{0:T(256)(128)(2,1)S(1)}, bf16[128]{0:T(256)(128)(2,1)}, u32[]{:S(2)}) copy-start(bf16[128]{0:T(256)(128)(2,1)} %param.11) | copy-start | bytes 772
  19.0 11.8 %all-to-all-start = ((f32[8,1,8192]{2,1,0:T(1,128)}), f32[8,1,8192]{2,1,0:T(1,128)S(1)}, u32[]{:S(2)}, u32[]{:S(2)}) async-start(f32[8,1,8192]{2,1,0:T(1,128)} %broadcast_in_dim.6), calls=%async_computation | async-start | bytes 524288 | tf_op jit(solution)/shard_map/all_to_all | solution.py:20
  70.8 21.5 %copy-start.1 = (f32[4,1024,128]{2,1,0:T(8,128)S(1)}, f32[4,1024,128]{2,1,0:T(8,128)}, u32[]{:S(2)}) copy-start(f32[4,1024,128]{2,1,0:T(8,128)} %get-tuple-element.44) | copy-start | bytes 6291460
  80.7 27.3 %all-to-all-start.2 = ((f32[16,1,4224]{2,1,0:T(1,128)}), f32[16,1,4224]{2,1,0:T(1,128)S(1)}, u32[]{:S(2)}, u32[]{:S(2)}) async-start(f32[16,1,4224]{2,1,0:T(1,128)} %broadcast_in_dim.8), calls=%async_computation.2 | async-start | bytes 540672 | tf_op jit(solution)/shard_map/all_to_all | solution.py:20
  91.0 25.8 %collective-permute-start.1 = (f32[4,30,128]{2,1,0:T(8,128)}, f32[4,30,128]{2,1,0:T(8,128)}, u32[]{:S(2)}, u32[]{:S(2)}) collective-permute-start(f32[4,30,128]{2,1,0:T(8,128)} %slice.593), channel_id=1, source_target_pairs={{8,0},{16,8},{24,16},{32,24},{40,32},{48,40},{56,48},{64,56},{72,6... | collective-permute-start | bytes 184328 | tf_op jit(solution)/shard_map/ppermute | solution.py:15
  108.0 25.1 %all-to-all-start.3 = ((bf16[16,8,4096]{2,1,0:T(8,128)(2,1)}), bf16[16,8,4096]{2,1,0:T(8,128)(2,1)}, u32[]{:S(2)}, u32[]{:S(2)}) async-start(bf16[16,8,4096]{2,1,0:T(8,128)(2,1)} %fusion.1), calls=%async_computation.3 | async-start | bytes 2097152 | tf_op jit(solution)/shard_map/all_to_all | solution.py:45
  (35 other events, 170.9 us)
where the time goes:
time: 136 us; the launch traced here: 135 us
  other arithmetic  39.6 us (29%)
  matrix products  31.5 us (23%)
  starting transfers between devices  26.7 us (20%)
  waiting for transfers between devices  19 us (14%)
  blocking collectives  9.92 us (7%)
  local copies, waits for them, and re-layouts  6.61 us (5%)
  between operations  1.8 us (1%)
    dot_general x1, matrix products, on_device(): jnp.einsum('std,cd->stc', out_grad, out_weight, preferred_element_type=jn...  17.5 us
    dot_general x1, matrix products, on_device(): lax.dot_general(flat_swished, flat_cot, (((0,), (0,)), ((), ())), preferr...  14 us
    all_to_all x2, starting transfers between devices, sent_to_all(): lax.all_to_all(jnp.broadcast_to(shard[None], (devices, *shard.shape)), ax...  13.1 us
    reduce_sum x2, other arithmetic, on_device(): jnp.sum(conv_grad * padded[:, tap_index:tap_index + tok_rows], axis=(0, 1))  11.3 us
    all_to_all x1, waiting for transfers between devices, sent_and_summed(): lax.all_to_all(pieces, axis, split_axis=0, concat_axis=0, tiled=True)  10.3 us
    all_to_all x1, blocking collectives, sent_to_all(): lax.all_to_all(jnp.broadcast_to(shard[None], (devices, *shard.shape)), ax...  9.92 us
    reduce_sum x1, other arithmetic, on_device(): jnp.sum(conv, axis=-1)  9.57 us
    add x1, other arithmetic, on_device(): spread + tap_rows[tap_index] * wide_grad[:, begin:begin + tok_rows + reach]  8.97 us
  transfers between devices with their start and end apart: 5, of which 3 were waited for; matrix products, arithmetic and copies ran while one was open for 17% of the time, Pallas kernels for 0%

commit v1 on v0

v1 whole, which is shorter than its diff:
```python
import functools

import jax
import jax.numpy as jnp
from jax import lax
from jax.experimental import pallas as pl
from jax.experimental.pallas import tpu as pltpu
from jax.sharding import PartitionSpec as P


K = 31
REACH = K - 1
PAD = 32
EPS = 1e-05
LANES = 128
F32 = jnp.float32
BF16 = jnp.bfloat16


def sigmoid(x):
    return 0.5 * jnp.tanh(0.5 * x) + 0.5


def taps_by_shift(first):
    groups = {}
    for tap in range(K):
        groups.setdefault(first(tap) % 8, []).append((tap, first(tap) // 8 * 8))
    return sorted(groups.items())


def conv_kernel(
    blocks, v_ref, g_ref, halo_ref, taps_ref, bias_ref,
    conv_ref, pay_ref, gated_ref, wide, tapf, rows,
):
    seq = pl.program_id(0)

    @pl.when(seq == 0)
    def _():
        tapf[:K] = taps_ref[...].astype(F32)

    gated_ref[0, :PAD] = halo_ref[0]
    wide[:PAD] = halo_ref[0].astype(F32)
    for b in range(blocks):
        at = b * LANES
        y = v_ref[0, at : at + LANES].astype(F32) * sigmoid(g_ref[0, at : at + LANES].astype(F32))
        y = y.astype(BF16)
        gated_ref[0, PAD + at : PAD + at + LANES] = y
        wide[PAD + at : PAD + at + LANES] = y.astype(F32)
    bias = bias_ref[...].astype(F32)

    def block(b, carry):
        at = b * LANES
        acc = jnp.broadcast_to(bias, (LANES, LANES))
        for shift, taps in taps_by_shift(lambda tap: tap + PAD - REACH):
            piece = wide[pl.ds(at + shift, LANES + taps[-1][1]), :]
            for tap, skip in taps:
                acc = acc + tapf[tap : tap + 1] * piece[skip : skip + LANES]
        turned = acc.T
        conv_ref[:, pl.ds(pl.multiple_of(at, LANES), LANES)] = turned
        mean = jnp.sum(turned, axis=0, keepdims=True) * (1.0 / LANES)
        off = turned - mean
        row = seq * blocks + b
        rows[pl.ds(row, 1)] = mean
        rows[pl.ds(row + rows.shape[0] // 2, 1)] = jnp.sum(off * off, axis=0, keepdims=True)
        return carry

    lax.fori_loop(0, blocks, block, 0, unroll=4)

    @pl.when(seq == pl.num_programs(0) - 1)
    def _():
        for peer in range(pay_ref.shape[0]):
            pay_ref[peer] = rows[...]


def swish_kernel(
    core_ref, w_hbm, w2_hbm, og_hbm, after_ref, mine_hbm, other_hbm,
    lhs, og, mine, other, wsem, sems, osems,
):
    n, tok, _ = og.shape
    chans = mine.shape[0]
    base = core_ref[0] * (n * tok)
    ins = []
    for i in range(n):
        at = pl.multiple_of(base + i * tok, tok)
        ins.append(pltpu.make_async_copy(og_hbm.at[pl.ds(at, tok)], og.at[i], sems.at[i]))
    weights = [
        pltpu.make_async_copy(w_hbm, lhs.at[pl.ds(0, chans)], wsem.at[0]),
        pltpu.make_async_copy(w2_hbm, lhs.at[pl.ds(chans, chans)], wsem.at[1]),
    ]
    for c in weights + ins:
        c.start()
    for c in weights:
        c.wait()
    outs = []
    for i in range(n):
        ins[i].wait()
        here = pl.ds(i * tok, tok)
        out = lax.dot_general(
            lhs[...], og[i], (((1,), (1,)), ((), ())), preferred_element_type=F32
        )
        mine[:, here] = out[:chans]
        other[:, here] = out[chans:].astype(BF16)
        outs += [
            pltpu.make_async_copy(mine.at[:, here], mine_hbm.at[:, here], osems.at[2 * i]),
            pltpu.make_async_copy(other.at[:, here], other_hbm.at[:, here], osems.at[2 * i + 1]),
        ]
        for c in outs[-2:]:
            c.start()
    for c in outs:
        c.wait()


def norm_kernel(
    core_ref, conv_ref, mine_ref, other_ref, got_ref, gain_ref,
    sw_ref, ng_ref, pay_ref, stat_ref, gg_ref, gcol, gacc, rows,
):
    step = pl.program_id(0)
    half = rows.shape[0] // 2
    peers = got_ref.shape[0]

    @pl.when(step == 0)
    def _():
        gain = jnp.broadcast_to(gain_ref[...].astype(F32), (LANES, LANES))
        gcol[...] = gain.T
        gacc[...] = jnp.zeros_like(gacc)
        mean = got_ref[0, :half]
        m2 = got_ref[0, half:]
        for p in range(1, peers):
            mean = mean + got_ref[p, :half]
            m2 = m2 + got_ref[p, half:]
        mean = mean * (1.0 / peers)
        apart = jnp.square(got_ref[0, :half] - mean)
        for p in range(1, peers):
            apart = apart + jnp.square(got_ref[p, :half] - mean)
        var = (m2 + LANES * apart) * (1.0 / (peers * LANES))
        stat_ref[:half] = mean
        stat_ref[half:] = lax.rsqrt(var + EPS)

    chunk = 32
    steps = pl.num_programs(0)
    seq = lax.rem(step + core_ref[0] * (steps // 2), steps)
    is_mine = step < steps // 2
    for j in range(conv_ref.shape[1] // LANES):
        at = j * LANES
        row = seq * (conv_ref.shape[1] // LANES) + j
        mean = stat_ref[pl.ds(row, 1)]
        inverse = stat_ref[pl.ds(half + row, 1)]
        s1 = jnp.zeros((8, LANES), F32)
        s2 = jnp.zeros((8, LANES), F32)
        for c in range(0, LANES, chunk):
            normed = (conv_ref[c : c + chunk, at : at + LANES] - mean) * inverse
            gain = gcol[c : c + chunk]
            scaled = normed * gain
            sig = sigmoid(scaled)
            sw_ref[c : c + chunk, at : at + LANES] = (scaled * sig).astype(BF16)
            swg = jnp.where(
                is_mine,
                mine_ref[c : c + chunk, at : at + LANES],
                other_ref[c : c + chunk, at : at + LANES].astype(F32),
            )
            sg = swg * sig * (1.0 + scaled * (1.0 - sig))
            gacc[c : c + chunk] += sg * normed
            ng = sg * gain
            ng_ref[c : c + chunk, at : at + LANES] = ng
            nn = ng * normed
            for r in range(0, chunk, 8):
                s1 = s1 + ng[r : r + 8]
                s2 = s2 + nn[r : r + 8]
        rows[pl.ds(row, 1)] = jnp.sum(s1, axis=0, keepdims=True)
        rows[pl.ds(half + row, 1)] = jnp.sum(s2, axis=0, keepdims=True)

    @pl.when(step == pl.num_programs(0) - 1)
    def _():
        gg_ref[...] = jnp.sum(gacc[...].T, axis=0, keepdims=True)
        for peer in range(peers):
            pay_ref[peer] = rows[...]


def weight_kernel(
    core_ref, sw_hbm, sw2_hbm, og_hbm, mine_hbm, other_hbm, lhs, og, mine, other, wsem, sems, osems
):
    n, _, cols = og.shape
    chans = lhs.shape[0] // 2
    base = core_ref[0] * (n * cols)
    ins = []
    for i in range(n):
        at = pl.multiple_of(base + i * cols, cols)
        ins.append(pltpu.make_async_copy(og_hbm.at[:, pl.ds(at, cols)], og.at[i], sems.at[i]))
    sides = [
        pltpu.make_async_copy(sw_hbm, lhs.at[pl.ds(0, chans)], wsem.at[0]),
        pltpu.make_async_copy(sw2_hbm, lhs.at[pl.ds(chans, chans)], wsem.at[1]),
    ]
    for c in sides + ins:
        c.start()
    for c in sides:
        c.wait()
    outs = []
    for i in range(n):
        ins[i].wait()
        part = jnp.dot(lhs[...], og[i], preferred_element_type=F32).astype(BF16)
        mine[i] = part[:chans].reshape(mine.shape[1:])
        other[i] = part[chans:].reshape(other.shape[1:])
        here = pl.ds(i * cols, cols)
        outs += [
            pltpu.make_async_copy(mine.at[i], mine_hbm.at[:, :, here], osems.at[2 * i]),
            pltpu.make_async_copy(other.at[i], other_hbm.at[:, :, here], osems.at[2 * i + 1]),
        ]
        for c in outs[-2:]:
            c.start()
    for c in outs:
        c.wait()


def turn_kernel(
    blocks, conv_ref, ng_ref, stat_ref, got_ref, cg_ref, head_ref, bias_ref, bias_acc, means
):
    seq = pl.program_id(0)
    half = stat_ref.shape[0] // 2
    peers = got_ref.shape[0]
    total = peers * LANES

    @pl.when(seq == 0)
    def _():
        s = got_ref[0]
        for p in range(1, peers):
            s = s + got_ref[p]
        means[...] = s * (1.0 / total)
        bias_acc[...] = jnp.zeros_like(bias_acc)

    for b in range(blocks):
        here = slice(b * LANES, (b + 1) * LANES)
        row = seq * blocks + b
        mean = stat_ref[pl.ds(row, 1)]
        inverse = stat_ref[pl.ds(half + row, 1)]
        m1 = means[pl.ds(row, 1)]
        m2 = means[pl.ds(half + row, 1)]
        normed = (conv_ref[:, here] - mean) * inverse
        cg = inverse * (ng_ref[:, here] - m1 - normed * m2)
        cg = cg.T
        cg_ref[0, here, :] = cg
        part = cg[:8]
        for r in range(8, LANES, 8):
            part = part + cg[r : r + 8]
        bias_acc[...] += part
        if b == 0:
            head_ref[0] = cg[:PAD]

    @pl.when(seq == pl.num_programs(0) - 1)
    def _():
        bias_ref[...] = jnp.sum(bias_acc[...], axis=0, keepdims=True)


def taps_kernel(
    blocks, cg_ref, gated_ref, gg_ref, bias_ref, got_hbm, pay_in,
    pay_ref, wide, taps_acc, small, came, sem, csems,
):
    seq = pl.program_id(0)
    at = came.shape[2]
    take = pltpu.make_async_copy(got_hbm, came, csems.at[0])
    put = pltpu.make_async_copy(came, pay_ref.at[:, :, pl.ds(at, at)], csems.at[1])

    @pl.when(seq == 0)
    def _():
        take.start()
        taps_acc[...] = jnp.zeros_like(taps_acc)

    @pl.when(seq == 1)
    def _():
        take.wait()
        put.start()

    wide[...] = gated_ref[0].astype(F32)

    def block(b, carry):
        at = b * LANES
        cg = cg_ref[0, pl.ds(pl.multiple_of(at, LANES), LANES), :]
        for shift, taps in taps_by_shift(lambda tap: tap + PAD - REACH):
            piece = wide[pl.ds(at + shift, LANES + taps[-1][1]), :]
            for tap, skip in taps:
                acc = taps_acc[tap]
                for r in range(0, LANES, 8):
                    acc = acc + cg[r : r + 8] * piece[skip + r : skip + r + 8]
                taps_acc[tap] = acc
        return carry

    lax.fori_loop(0, blocks, block, 0, unroll=2)

    @pl.when(seq == pl.num_programs(0) - 1)
    def _():
        rows = [jnp.sum(taps_acc[tap], axis=0, keepdims=True) for tap in range(K)]
        rows += [gg_ref[...], bias_ref[...]]
        rows += [jnp.zeros((1, LANES), F32)] * (-len(rows) % 8)
        for t in range(len(rows) // 8):
            tile = jnp.concatenate(rows[8 * t : 8 * t + 8], axis=0).astype(BF16)
            for peer in range(small.shape[0]):
                small[peer, :, t * LANES : (t + 1) * LANES] = tile
        copy = pltpu.make_async_copy(
            small, pay_ref.at[:, :, pl.ds(2 * at, small.shape[2])], sem
        )
        copy.start()
        copy.wait()
        put.wait()


def spread_kernel(blocks, cg_ref, next_ref, v_ref, g_ref, taps_ref, vg_ref, gg_ref, wide, tapf):
    @pl.when(pl.program_id(0) == 0)
    def _():
        tapf[:K] = taps_ref[...].astype(F32)

    length = blocks * LANES
    wide[:length] = cg_ref[0]
    wide[length : length + PAD] = next_ref[0]

    def block(b, carry):
        at = b * LANES
        acc = None
        for shift, taps in taps_by_shift(lambda tap: REACH - tap):
            piece = wide[pl.ds(at + shift, LANES + max(skip for _, skip in taps)), :]
            for tap, skip in taps:
                term = tapf[tap : tap + 1] * piece[skip : skip + LANES]
                acc = term if acc is None else acc + term
        here = pl.ds(pl.multiple_of(at, LANES), LANES)
        sig = sigmoid(g_ref[0, here, :].astype(F32))
        v = v_ref[0, here, :].astype(F32)
        vg = acc * sig
        vg_ref[0, here, :] = vg.astype(BF16)
        gg_ref[0, here, :] = (vg * v * (1.0 - sig)).astype(BF16)
        return carry

    lax.fori_loop(0, blocks, block, 0, unroll=4)


def final_kernel(core_ref, got_ref, w_ref, taps_ref, gain_ref, bias_ref):
    acc = got_ref[0].astype(F32)
    for p in range(1, got_ref.shape[0]):
        acc = acc + got_ref[p].astype(F32)
    width = w_ref.shape[1]
    half = width // 2
    for side in range(2):
        at = pl.multiple_of((core_ref[0] + side) % 2 * half, half)
        w_ref[:, pl.ds(at, half)] = acc[:, side * half : (side + 1) * half]
    for t in range(K // 8 + 1):
        tile = acc[:, width + t * LANES : width + (t + 1) * LANES]
        taps_ref[8 * t : min(8 * t + 8, K)] = tile[: min(8, K - 8 * t)]
    for ref, row in ((gain_ref, K), (bias_ref, K + 1)):
        at = width + row // 8 * LANES
        ref[...] = acc[row % 8 : row % 8 + 1, at : at + LANES]


def whole(shape):
    return pl.BlockSpec(shape, lambda i: (0,) * len(shape))


PARAMS = pltpu.CompilerParams(vmem_limit_bytes=67_000_000)


def cost(flops, moved):
    return pl.CostEstimate(flops=flops, bytes_accessed=moved, transcendentals=0)


def on_device(values_in, gates_in, conv_taps, conv_bias, norm_gain, out_weight, out_grad):
    seqs, length, chans = values_in.shape
    width = out_grad.shape[2]
    tokens = seqs * length
    blocks = length // LANES
    tp, sp = lax.axis_size("tp"), lax.axis_size("sp")
    stat_rows = 2 * tokens // LANES
    flat = out_grad.reshape(tokens, width)
    ahead = [(i, i + 1) for i in range(sp - 1)]
    back = [(i + 1, i) for i in range(sp - 1)]
    swap = [(i, i ^ 1) for i in range(tp)]
    core = (lax.axis_index("tp") % 2).astype(jnp.int32).reshape(1)
    bias_row = conv_bias.reshape(1, chans)
    gain_row = norm_gain.reshape(1, chans)

    SDS = jax.ShapeDtypeStruct
    any_ = pl.BlockSpec(memory_space=pl.ANY)
    vmem = pl.BlockSpec(memory_space=pltpu.VMEM)
    smem = pl.BlockSpec(memory_space=pltpu.SMEM)
    seq_block = pl.BlockSpec((1, length, chans), lambda i: (i, 0, 0))
    head_block = pl.BlockSpec((1, PAD, chans), lambda i: (i, 0, 0))
    gated_block = pl.BlockSpec((1, length + PAD, chans), lambda i: (i, 0, 0))
    col = pl.BlockSpec((chans, length), lambda i: (0, i))
    stats = whole((tp, stat_rows, LANES))

    tail = slice(length - PAD, length)
    edge = values_in[:, tail].astype(F32) * sigmoid(gates_in[:, tail].astype(F32))
    halo = lax.ppermute(edge.astype(BF16), "sp", ahead)
    weight2 = lax.ppermute(out_weight, "tp", swap)
    conv, pay, gated = pl.pallas_call(
        functools.partial(conv_kernel, blocks),
        grid=(seqs,),
        in_specs=[seq_block, seq_block, head_block, whole((K, chans)), whole((1, chans))],
        out_specs=[col, stats, gated_block],
        out_shape=[
            SDS((chans, tokens), F32),
            SDS((tp, stat_rows, LANES), F32),
            SDS((seqs, length + PAD, chans), BF16),
        ],
        scratch_shapes=[
            pltpu.VMEM((length + 2 * PAD, chans), F32),
            pltpu.VMEM((PAD, chans), F32),
            pltpu.VMEM((stat_rows, LANES), F32),
        ],
        compiler_params=PARAMS,
        cost_estimate=cost(2 * K * tokens * chans, 8 << 20),
        name="conv",
    )(values_in, gates_in, halo, conv_taps, bias_row)
    got = lax.all_to_all(pay, "tp", 0, 0, tiled=True)

    pieces = 4
    mine, other = pl.pallas_call(
        swish_kernel,
        in_specs=[smem, any_, any_, any_, any_],
        out_specs=[any_, any_],
        out_shape=[SDS((chans, tokens // 2), F32), SDS((chans, tokens // 2), BF16)],
        scratch_shapes=[
            pltpu.VMEM((2 * chans, width), BF16),
            pltpu.VMEM((pieces, tokens // 2 // pieces, width), BF16),
            pltpu.VMEM((chans, tokens // 2), F32),
            pltpu.VMEM((chans, tokens // 2), BF16),
            pltpu.SemaphoreType.DMA((2,)),
            pltpu.SemaphoreType.DMA((pieces,)),
            pltpu.SemaphoreType.DMA((2 * pieces,)),
        ],
        compiler_params=PARAMS,
        cost_estimate=cost(2 * tokens * chans * width, tokens * width),
        name="swish_grad",
    )(core, out_weight, weight2, flat, pay)
    other = lax.ppermute(other, "tp", swap)

    half = seqs // 2
    turned = pl.BlockSpec((chans, length), lambda i, c: (0, (i + c[0] * half) % seqs))
    swished, ng, pay2, stat, gg = pl.pallas_call(
        norm_kernel,
        grid_spec=pltpu.PrefetchScalarGridSpec(
            num_scalar_prefetch=1,
            grid=(seqs,),
            in_specs=[
                turned,
                pl.BlockSpec((chans, length), lambda i, c: (0, jnp.minimum(i, half - 1))),
                pl.BlockSpec((chans, length), lambda i, c: (0, jnp.maximum(i, half) - half)),
                pl.BlockSpec((tp, stat_rows, LANES), lambda i, c: (0, 0, 0)),
                pl.BlockSpec((1, chans), lambda i, c: (0, 0)),
            ],
            out_specs=[
                turned,
                turned,
                pl.BlockSpec((tp, stat_rows, LANES), lambda i, c: (0, 0, 0)),
                pl.BlockSpec((stat_rows, LANES), lambda i, c: (0, 0)),
                pl.BlockSpec((1, chans), lambda i, c: (0, 0)),
            ],
            scratch_shapes=[
                pltpu.VMEM((chans, LANES), F32),
                pltpu.VMEM((chans, LANES), F32),
                pltpu.VMEM((stat_rows, LANES), F32),
            ],
        ),
        out_shape=[
            SDS((chans, tokens), BF16),
            SDS((chans, tokens), F32),
            SDS((tp, stat_rows, LANES), F32),
            SDS((stat_rows, LANES), F32),
            SDS((1, chans), F32),
        ],
        compiler_params=PARAMS,
        cost_estimate=cost(30 * tokens * chans, 8 << 20),
        name="norm",
    )(core, conv, mine, other, got, gain_row)
    swished2 = lax.ppermute(swished, "tp", swap)
    got2 = lax.all_to_all(pay2, "tp", 0, 0, tiled=True)

    extra = -(-(K + 2) // 8) * LANES
    cols = width // 2 // pieces
    part = (sp, chans // sp, width // 2)
    pay3, other_w = pl.pallas_call(
        weight_kernel,
        in_specs=[smem, any_, any_, any_],
        out_specs=[any_, any_],
        out_shape=[SDS((sp, chans // sp, width + extra), BF16), SDS(part, BF16)],
        scratch_shapes=[
            pltpu.VMEM((2 * chans, tokens), BF16),
            pltpu.VMEM((pieces, tokens, cols), BF16),
            pltpu.VMEM((pieces, sp, chans // sp, cols), BF16),
            pltpu.VMEM((pieces, sp, chans // sp, cols), BF16),
            pltpu.SemaphoreType.DMA((2,)),
            pltpu.SemaphoreType.DMA((pieces,)),
            pltpu.SemaphoreType.DMA((2 * pieces,)),
        ],
        compiler_params=PARAMS,
        cost_estimate=cost(2 * tokens * chans * width, tokens * width),
        name="weight_grad",
    )(core, swished, swished2, flat)
    other_w = lax.ppermute(other_w, "tp", swap)

    cg, head, bias_local = pl.pallas_call(
        functools.partial(turn_kernel, blocks),
        grid=(seqs,),
        in_specs=[col, col, whole((stat_rows, LANES)), stats],
        out_specs=[seq_block, head_block, whole((1, chans))],
        out_shape=[
            SDS((seqs, length, chans), F32),
            SDS((seqs, PAD, chans), F32),
            SDS((1, chans), F32),
        ],
        scratch_shapes=[pltpu.VMEM((8, chans), F32), pltpu.VMEM((stat_rows, LANES), F32)],
        compiler_params=PARAMS,
        cost_estimate=cost(30 * tokens * chans, 8 << 20),
        name="conv_grad",
    )(conv, ng, stat, got2)
    after = lax.ppermute(head, "sp", back)

    pay3 = pl.pallas_call(
        functools.partial(taps_kernel, blocks),
        grid=(seqs,),
        in_specs=[seq_block, gated_block, whole((1, chans)), whole((1, chans)), any_, any_],
        out_specs=any_,
        out_shape=SDS(pay3.shape, BF16),
        scratch_shapes=[
            pltpu.VMEM((length + PAD, chans), F32),
            pltpu.VMEM((K, 8, chans), F32),
            pltpu.VMEM((sp, chans // sp, extra), BF16),
            pltpu.VMEM(part, BF16),
            pltpu.SemaphoreType.DMA,
            pltpu.SemaphoreType.DMA((2,)),
        ],
        input_output_aliases={5: 0},
        compiler_params=PARAMS,
        cost_estimate=cost(2 * K * tokens * chans, 8 << 20),
        name="taps_grad",
    )(cg, gated, gg, bias_local, other_w, pay3)
    got3 = lax.all_to_all(pay3, "sp", 0, 0, tiled=True)

    values_grad, gates_grad = pl.pallas_call(
        functools.partial(spread_kernel, blocks),
        grid=(seqs,),
        in_specs=[seq_block, head_block, seq_block, seq_block, whole((K, chans))],
        out_specs=[seq_block, seq_block],
        out_shape=[SDS((seqs, length, chans), BF16)] * 2,
        scratch_shapes=[pltpu.VMEM((length + 2 * PAD, chans), F32), pltpu.VMEM((PAD, chans), F32)],
        compiler_params=PARAMS,
        cost_estimate=cost(2 * K * tokens * chans, 8 << 20),
        name="gated_grad",
    )(cg, after, values_in, gates_in, conv_taps)

    weight_grad, taps_grad, gain_grad, bias_grad = pl.pallas_call(
        final_kernel,
        in_specs=[smem, vmem],
        out_specs=[vmem] * 4,
        out_shape=[
            SDS((chans // sp, width), F32),
            SDS((K, chans), F32),
            SDS((1, chans), F32),
            SDS((1, chans), F32),
        ],
        compiler_params=PARAMS,
        name="final_sum",
    )(core, got3)
    gain_grad, bias_grad = gain_grad.reshape(chans), bias_grad.reshape(chans)
    return values_grad, gates_grad, taps_grad, gain_grad, bias_grad, weight_grad


def solution(mesh):
    return jax.shard_map(
        on_device,
        mesh=mesh,
        in_specs=(
            P(None, "sp", "tp"),
            P(None, "sp", "tp"),
            P(None, "tp"),
            P("tp"),
            P("tp"),
            P("tp", None),
            P(None, "sp", None),
        ),
        out_specs=(
            P(None, "sp", "tp"),
            P(None, "sp", "tp"),
            P(None, "tp"),
            P("tp"),
            P("tp"),
            P(("tp", "sp"), None),
        ),
        check_vma=False,
    )
```

time: 136 us -> 118 us (0.87)
  Pallas kernels: 0 us -> 57.2 us
  other arithmetic: 39.6 us -> 0.8 us
  matrix products: 31.5 us -> 0 us
  blocking collectives: 9.92 us -> 23.6 us
  starting transfers between devices: 26.7 us -> 14.3 us
  local copies, waits for them, and re-layouts: 6.61 us -> 0.62 us
    pallas_call x0 -> x8, Pallas kernels: none -> 57.2 us  [the longest x1 11.1 us: on_device(): pl.pallas_call(swish_kernel, in_specs=[smem, any_, any_, any_, any_], out...]
    dot_general x2 -> x0, matrix products: 31.5 us -> none  [the longest x1 17.5 us: on_device(): jnp.einsum('std,cd->stc', out_grad, out_weight, preferred_element_type=jn...]
    reduce_sum x7 -> x0, other arithmetic: 23.5 us -> none  [the longest x2 11.3 us: on_device(): jnp.sum(conv_grad * padded[:, tap_index:tap_index + tok_rows], axis=(0, 1))]
    ppermute x2 -> x6, waiting for transfers between devices: 1.21 us -> 19.7 us  [the longest x1 15.1 us: on_device(): after = lax.ppermute(head, 'sp', back)]
    all_to_all x3 -> x1, waiting for transfers between devices: 17.8 us -> 0.01 us  [on_device(): got3 = lax.all_to_all(pay3, 'sp', 0, 0, tiled=True)]
    all_to_all x1 -> x2, blocking collectives: 9.92 us -> 23.6 us  [the longest x1 12 us: on_device(): got = lax.all_to_all(pay, 'tp', 0, 0, tiled=True)]
    all_to_all x3 -> x1, starting transfers between devices: 21.8 us -> 8.97 us  [on_device(): got3 = lax.all_to_all(pay3, 'sp', 0, 0, tiled=True)]
    add x2 -> x0, other arithmetic: 9.86 us -> none  [the longest x1 8.97 us: on_device(): spread + tap_rows[tap_index] * wide_grad[:, begin:begin + tok_rows + reach]]
  transfers between devices with their start and end apart: 5 -> 7, of which waited for: 3 -> 3; matrix products, arithmetic and copies ran while one was open for 17% -> 1% of each run, Pallas kernels for 0% -> 18%
where the time goes in v1:
time: 118 us; the launch traced here: 117 us
  Pallas kernels  57.2 us (48%)
  blocking collectives  23.6 us (20%)
  waiting for transfers between devices  19.7 us (17%)
  starting transfers between devices  14.3 us (12%)
    ppermute x1, waiting for transfers between devices, on_device(): after = lax.ppermute(head, 'sp', back)  15.1 us
    all_to_all x1, blocking collectives, on_device(): got = lax.all_to_all(pay, 'tp', 0, 0, tiled=True)  12 us
    all_to_all x1, blocking collectives, on_device(): got2 = lax.all_to_all(pay2, 'tp', 0, 0, tiled=True)  11.5 us
    pallas_call x1, Pallas kernels, on_device(): pl.pallas_call(swish_kernel, in_specs=[smem, any_, any_, any_, any_], out...  11.1 us
    pallas_call x1, Pallas kernels, on_device(): pl.pallas_call(weight_kernel, in_specs=[smem, any_, any_, any_], out_spec...  11 us
    all_to_all x1, starting transfers between devices, on_device(): got3 = lax.all_to_all(pay3, 'sp', 0, 0, tiled=True)  8.97 us
    pallas_call x1, Pallas kernels, on_device(): pl.pallas_call(functools.partial(conv_kernel, blocks), grid=(seqs,), in_s...  8.3 us
    pallas_call x1, Pallas kernels, on_device(): pl.pallas_call(functools.partial(spread_kernel, blocks), grid=(seqs,), in...  7.63 us
  transfers between devices with their start and end apart: 7, of which 3 were waited for; matrix products, arithmetic and copies ran while one was open for 1% of the time, Pallas kernels for 18%

profile of v1, /device:TPU:0, one launch (start us, length us, event | category | flops | bytes accessed | tf_op | source)
XLA Modules:
  0.0 116.8 jit_solution(5669157180839713510)
XLA Ops:
  0.6 0.1 collective-permute-start.1
  0.7 0.8 multiply_convert_fusion
  1.5 3.6 %collective-permute-start = (bf16[4,32,128]{2,1,0:T(8,128)(2,1)S(1)}, bf16[4,32,128]{2,1,0:T(8,128)(2,1)S(1)}, u32[]{:S(2)}, u32[]{:S(2)}) collective-permute-start(bf16[4,32,128]{2,1,0:T(8,128)(2,1)S(1)} %multiply_convert_fusion), channel_id=1, source_target_pairs={{0,8},{8,16},{16,24},{24,32},{32,40},{40,48},{48,56},{56,64},{64,7... | collective-permute-start | bytes 98312 | tf_op jit(solution)/shard_map/ppermute | solution.py:388
  5.1 1.6 %collective-permute-done.halo_ref = bf16[4,32,128]{2,1,0:T(8,128)(2,1)S(1)} collective-permute-done((bf16[4,32,128]{2,1,0:T(8,128)(2,1)S(1)}, bf16[4,32,128]{2,1,0:T(8,128)(2,1)S(1)}, u32[]{:S(2)}, u32[]{:S(2)}) %collective-permute-start) | collective-permute-done | bytes 32800 | tf_op jit(solution)/shard_map/ppermute | solution.py:388
  6.7 0.0 copy-start
  6.7 0.6 copy-done
  7.3 8.3 %conv.1 = (f32[128,4096]{1,0:T(8,128)}, f32[8,64,128]{2,1,0:T(8,128)}, bf16[4,1056,128]{2,1,0:T(8,128)(2,1)}) custom-call(bf16[4,1024,128]{2,1,0:T(8,128)(2,1)} %v_ref.3, bf16[4,1024,128]{2,1,0:T(8,128)(2,1)} %g_ref.3, bf16[4,32,128]{2,1,0:T(8,128)(2,1)} %copy-done, bf16[31,128]{1,0:T(8,128)(2,1)} %taps_ref.3, bf16[1,128]{1,0:T(2,128)(2,1)} %bitcast.8), custom_call_target="tpu_custom_call" | custom-call | flops 32505856 | bytes 8388608 | tf_op jit(solution)/shard_map/conv/pallas_call | solution.py:390
  15.6 0.0 collective-permute-done.1.w2_hbm
  15.6 11.1 %swish_grad.1 = (f32[128,2048]{1,0:T(8,128)}, bf16[128,2048]{1,0:T(8,128)(2,1)}) custom-call(s32[1]{0:T(128)} %bitcast.1.core_ref, bf16[128,4096]{1,0:T(8,128)(2,1)} %w_hbm.1, bf16[128,4096]{1,0:T(8,128)(2,1)} %collective-permute-done.1.w2_hbm, bf16[4096,4096]{1,0:T(8,128)(2,1)} %bitcast.6, f32[8,64,128]{2,1,0:T(8,128)} %get-tuple-element.28.after_ref), custom_call_target="tpu_custom_call" | custom-call | flops 4294967296 | bytes 16777216 | tf_op jit(solution)/shard_map/swish_grad/pallas_call | solution.py:412
  26.8 0.1 collective-permute-start.2
  26.9 12.0 %all_to_all.15.got_ref = f32[8,64,128]{2,1,0:T(8,128)} all-to-all(f32[8,64,128]{2,1,0:T(8,128)} %get-tuple-element.28.after_ref), channel_id=1, replica_groups=mesh['sp'=16,'tp'=8] {'tp'}, dimensions={0} | all-to-all | bytes 524288 | tf_op jit(solution)/shard_map/all_to_all | solution.py:409
  38.9 0.0 collective-permute-done.2.other_ref
  38.9 5.7 %norm.1 = (bf16[128,4096]{1,0:T(8,128)(2,1)}, f32[128,4096]{1,0:T(8,128)}, f32[8,64,128]{2,1,0:T(8,128)}, f32[64,128]{1,0:T(8,128)}, f32[1,128]{1,0:T(1,128)}) custom-call(s32[1]{0:T(128)} %bitcast.1.core_ref, f32[128,4096]{1,0:T(8,128)} %get-tuple-element.27.conv_ref, f32[128,2048]{1,0:T(8,128)} %get-tuple-element.29.mine_ref, ...), custom_call_target="tpu_custom_call" | custom-call | flops 15728640 | bytes 8388608 | tf_op jit(solution)/shard_map/norm/pallas_call | solution.py:434
  44.6 0.0 collective-permute-start.4
  44.6 3.0 %collective-permute-done.4.sw2_hbm = bf16[128,4096]{1,0:T(8,128)(2,1)} collective-permute-done((bf16[128,4096]{1,0:T(8,128)(2,1)}, bf16[128,4096]{1,0:T(8,128)(2,1)}, u32[]{:S(2)}, u32[]{:S(2)}) %collective-permute-start.4) | collective-permute-done | bytes 1048608 | tf_op jit(solution)/shard_map/ppermute | solution.py:470
  47.6 11.0 %weight_grad.1 = (bf16[16,8,4736]{2,1,0:T(8,128)(2,1)}, bf16[16,8,2048]{2,1,0:T(8,128)(2,1)}) custom-call(s32[1]{0:T(128)} %bitcast.1.core_ref, bf16[128,4096]{1,0:T(8,128)(2,1)} %get-tuple-element.41.sw_hbm, bf16[128,4096]{1,0:T(8,128)(2,1)} %collective-permute-done.4.sw2_hbm, bf16[4096,4096]{1,0:T(8,128)(2,1)} %bitcast.7), custom_call_target="tpu_custom_call" | custom-call | flops 4294967296 | bytes 16777216 | tf_op jit(solution)/shard_map/weight_grad/pallas_call | solution.py:476
  58.6 0.2 collective-permute-start.5
  58.8 11.5 %all_to_all.16.got_ref = f32[8,64,128]{2,1,0:T(8,128)} all-to-all(f32[8,64,128]{2,1,0:T(8,128)} %get-tuple-element.33), channel_id=1, replica_groups=mesh['sp'=16,'tp'=8] {'tp'}, dimensions={0} | all-to-all | bytes 524288 | tf_op jit(solution)/shard_map/all_to_all | solution.py:471
  70.3 4.6 %conv_grad.1 = (f32[4,1024,128]{2,1,0:T(8,128)}, f32[4,32,128]{2,1,0:T(8,128)}, f32[1,128]{1,0:T(1,128)}) custom-call(f32[128,4096]{1,0:T(8,128)} %get-tuple-element.27.conv_ref, f32[128,4096]{1,0:T(8,128)} %get-tuple-element.31.ng_ref, f32[64,128]{1,0:T(8,128)} %get-tuple-element.32.stat_ref, f32[8,64,128]{2,1,0:T(8,128)} %all_to_all.16.got_ref), custom_call_target="tpu_custom_call" | custom-call | flops 15728640 | bytes 8388608 | tf_op jit(solution)/shard_map/conv_grad/pallas_call | solution.py:496
  75.0 0.0 collective-permute-done.5.got_hbm
  75.0 6.7 %taps_grad.1 = bf16[16,8,4736]{2,1,0:T(8,128)(2,1)} custom-call(f32[4,1024,128]{2,1,0:T(8,128)} %get-tuple-element.34.cg_ref, bf16[4,1056,128]{2,1,0:T(8,128)(2,1)} %get-tuple-element.38.gated_ref, f32[1,128]{1,0:T(1,128)} %get-tuple-element.39.gg_ref, f32[1,128]{1,0:T(1,128)} %get-tuple-element.40.bias_ref, ...), custom_call_target="tpu_custom_call", output_to_operand_aliasing={{}: (5, {})} | custom-call | flops 32505856 | bytes 8388608 | tf_op jit(solution)/shard_map/taps_grad/pallas_call | solution.py:513
  81.7 0.0 copy-start.1
  81.7 9.0 %all-to-all-start.2 = ((bf16[16,8,4736]{2,1,0:T(8,128)(2,1)}), bf16[16,8,4736]{2,1,0:T(8,128)(2,1)}, u32[]{:S(2)}, u32[]{:S(2)}) async-start(bf16[16,8,4736]{2,1,0:T(8,128)(2,1)} %taps_grad.1), calls=%async_computation.2 | async-start | bytes 2424832 | tf_op jit(solution)/shard_map/all_to_all | solution.py:532
  90.7 0.0 copy-done.1
  90.7 1.3 %collective-permute-start.3 = (f32[4,32,128]{2,1,0:T(8,128)S(1)}, f32[4,32,128]{2,1,0:T(8,128)}, u32[]{:S(2)}, u32[]{:S(2)}) collective-permute-start(f32[4,32,128]{2,1,0:T(8,128)S(1)} %copy-done.1), channel_id=1, source_target_pairs={{8,0},{16,8},{24,16},{32,24},{40,32},{48,40},{56,48},{64,56},{72,6... | collective-permute-start | bytes 196616 | tf_op jit(solution)/shard_map/ppermute | solution.py:511
  92.0 15.1 %collective-permute-done.3.next_ref = f32[4,32,128]{2,1,0:T(8,128)} collective-permute-done((f32[4,32,128]{2,1,0:T(8,128)S(1)}, f32[4,32,128]{2,1,0:T(8,128)}, u32[]{:S(2)}, u32[]{:S(2)}) %collective-permute-start.3) | collective-permute-done | bytes 65568 | tf_op jit(solution)/shard_map/ppermute | solution.py:511
  107.1 7.6 %gated_grad.1 = (bf16[4,1024,128]{2,1,0:T(8,128)(2,1)}, bf16[4,1024,128]{2,1,0:T(8,128)(2,1)}) custom-call(f32[4,1024,128]{2,1,0:T(8,128)} %get-tuple-element.34.cg_ref, f32[4,32,128]{2,1,0:T(8,128)} %collective-permute-done.3.next_ref, bf16[4,1024,128]{2,1,0:T(8,128)(2,1)} %v_ref.3, bf16[4,1024,128]{2,1,0:T(8,128)(2,1)} %g_ref.3, bf16[31,128]{1,0:T(8,128)(2,1)} %taps_ref.3), custom_call_target="tpu_custom_call" | custom-call | flops 32505856 | bytes 8388608 | tf_op jit(solution)/shard_map/gated_grad/pallas_call | solution.py:534
  114.7 0.0 all-to-all-done.2.got_ref
  114.7 2.1 %final_sum.1 = (f32[8,4096]{1,0:T(8,128)}, f32[31,128]{1,0:T(8,128)}, f32[1,128]{1,0:T(1,128)}, f32[1,128]{1,0:T(1,128)}) custom-call(s32[1]{0:T(128)} %bitcast.1.core_ref, bf16[16,8,4736]{2,1,0:T(8,128)(2,1)} %all-to-all-done.2.got_ref), custom_call_target="tpu_custom_call" | custom-call | tf_op jit(solution)/shard_map/final_sum/pallas_call | solution.py:546
Async XLA Ops:
  0.6 15.0 %collective-permute-start.1 = (bf16[128,4096]{1,0:T(8,128)(2,1)}, bf16[128,4096]{1,0:T(8,128)(2,1)}, u32[]{:S(2)}, u32[]{:S(2)}) collective-permute-start(bf16[128,4096]{1,0:T(8,128)(2,1)} %w_hbm.1), channel_id=1, source_target_pairs={{0,1},{1,0},{2,3},{3,2},{4,5},{5,4},{6,7},{7,6},{8,9},{9,8},{10,11... | collective-permute-start | bytes 3145736 | tf_op jit(solution)/shard_map/ppermute | solution.py:389
  1.5 5.2 %collective-permute-start = (bf16[4,32,128]{2,1,0:T(8,128)(2,1)S(1)}, bf16[4,32,128]{2,1,0:T(8,128)(2,1)S(1)}, u32[]{:S(2)}, u32[]{:S(2)}) collective-permute-start(bf16[4,32,128]{2,1,0:T(8,128)(2,1)S(1)} %multiply_convert_fusion), channel_id=1, source_target_pairs={{0,8},{8,16},{16,24},{24,32},{32,40},{40,48},{48,56},{56,64},{64,7... | collective-permute-start | bytes 98312 | tf_op jit(solution)/shard_map/ppermute | solution.py:388
  6.7 0.6 copy-start
  26.8 12.1 %collective-permute-start.2 = (bf16[128,2048]{1,0:T(8,128)(2,1)}, bf16[128,2048]{1,0:T(8,128)(2,1)}, u32[]{:S(2)}, u32[]{:S(2)}) collective-permute-start(bf16[128,2048]{1,0:T(8,128)(2,1)} %get-tuple-element.30), channel_id=1, source_target_pairs={{0,1},{1,0},{2,3},{3,2},{4,5},{5,4},{6,7},{7,6},{8,9},{9,8},{10,11... | collective-permute-start | bytes 1572872 | tf_op jit(solution)/shard_map/ppermute | solution.py:430
  44.6 3.0 %collective-permute-start.4 = (bf16[128,4096]{1,0:T(8,128)(2,1)}, bf16[128,4096]{1,0:T(8,128)(2,1)}, u32[]{:S(2)}, u32[]{:S(2)}) collective-permute-start(bf16[128,4096]{1,0:T(8,128)(2,1)} %get-tuple-element.41.sw_hbm), channel_id=1, source_target_pairs={{0,1},{1,0},{2,3},{3,2},{4,5},{5,4},{6,7},{7,6},{8,9},{9,8},{10,11... | collective-permute-start | bytes 3145736 | tf_op jit(solution)/shard_map/ppermute | solution.py:470
  58.6 16.4 %collective-permute-start.5 = (bf16[16,8,2048]{2,1,0:T(8,128)(2,1)}, bf16[16,8,2048]{2,1,0:T(8,128)(2,1)}, u32[]{:S(2)}, u32[]{:S(2)}) collective-permute-start(bf16[16,8,2048]{2,1,0:T(8,128)(2,1)} %get-tuple-element.42), channel_id=1, source_target_pairs={{0,1},{1,0},{2,3},{3,2},{4,5},{5,4},{6,7},{7,6},{8,9},{9,8},{10,11... | collective-permute-start | bytes 1572872 | tf_op jit(solution)/shard_map/ppermute | solution.py:494
  81.7 9.0 %copy-start.1 = (f32[4,32,128]{2,1,0:T(8,128)S(1)}, f32[4,32,128]{2,1,0:T(8,128)}, u32[]{:S(2)}) copy-start(f32[4,32,128]{2,1,0:T(8,128)} %get-tuple-element.35) | copy-start | bytes 196612
  81.7 33.0 %all-to-all-start.2 = ((bf16[16,8,4736]{2,1,0:T(8,128)(2,1)}), bf16[16,8,4736]{2,1,0:T(8,128)(2,1)}, u32[]{:S(2)}, u32[]{:S(2)}) async-start(bf16[16,8,4736]{2,1,0:T(8,128)(2,1)} %taps_grad.1), calls=%async_computation.2 | async-start | bytes 2424832 | tf_op jit(solution)/shard_map/all_to_all | solution.py:532
  90.7 16.4 %collective-permute-start.3 = (f32[4,32,128]{2,1,0:T(8,128)S(1)}, f32[4,32,128]{2,1,0:T(8,128)}, u32[]{:S(2)}, u32[]{:S(2)}) collective-permute-start(f32[4,32,128]{2,1,0:T(8,128)S(1)} %copy-done.1), channel_id=1, source_target_pairs={{8,0},{16,8},{24,16},{32,24},{40,32},{48,40},{56,48},{64,56},{72,6... | collective-permute-start | bytes 196616 | tf_op jit(solution)/shard_map/ppermute | solution.py:511

commit v2 on v1

--- a/solution.py
+++ b/solution.py
@@ -29,14 +29,35 @@
 
 
 def conv_kernel(
-    blocks, v_ref, g_ref, halo_ref, taps_ref, bias_ref,
-    conv_ref, pay_ref, gated_ref, wide, tapf, rows,
+    blocks, core_ref, v_ref, g_ref, halo_ref, taps_ref, bias_ref, w_hbm, w2_hbm, og_hbm,
+    conv_ref, pay_ref, gated_ref, mine_ref, other_ref, wide, tapf, rows, lhs, og, wsem, sems,
 ):
     seq = pl.program_id(0)
+    n, tok, _ = og.shape
+    chans = mine_ref.shape[0]
+    base = core_ref[0] * (og_hbm.shape[0] // 2)
+
+    def fetch(i):
+        at = base + i // 2 * (blocks * LANES) + i % 2 * tok
+        return pltpu.make_async_copy(
+            og_hbm.at[pl.ds(pl.multiple_of(at, tok), tok)], og.at[i], sems.at[i]
+        )
+
+    weights = [
+        pltpu.make_async_copy(w_hbm, lhs.at[pl.ds(0, chans)], wsem.at[0]),
+        pltpu.make_async_copy(w2_hbm, lhs.at[pl.ds(chans, chans)], wsem.at[1]),
+    ]
 
     @pl.when(seq == 0)
     def _():
+        for c in weights:
+            c.start()
+        fetch(0).start()
         tapf[:K] = taps_ref[...].astype(F32)
+
+    @pl.when(seq < n - 1)
+    def _():
+        fetch(seq + 1).start()
 
     gated_ref[0, :PAD] = halo_ref[0]
     wide[:PAD] = halo_ref[0].astype(F32)
@@ -64,7 +85,19 @@
         rows[pl.ds(row + rows.shape[0] // 2, 1)] = jnp.sum(off * off, axis=0, keepdims=True)
         return carry
 
-    lax.fori_loop(0, blocks, block, 0, unroll=4)
+    lax.fori_loop(0, blocks // 2, block, 0, unroll=4)
+
+    @pl.when(seq == 0)
+    def _():
+        for c in weights:
+            c.wait()
+
+    fetch(seq).wait()
+    out = lax.dot_general(lhs[...], og[seq], (((1,), (1,)), ((), ())), preferred_element_type=F32)
+    mine_ref[...] = out[:chans]
+    other_ref[...] = out[chans:].astype(BF16)
+    for b in range(blocks // 2, blocks):
+        block(b, 0)
 
     @pl.when(seq == pl.num_programs(0) - 1)
     def _():
@@ -78,10 +111,10 @@
 ):
     n, tok, _ = og.shape
     chans = mine.shape[0]
-    base = core_ref[0] * (n * tok)
+    base = core_ref[0] * (2 * n * tok)
     ins = []
     for i in range(n):
-        at = pl.multiple_of(base + i * tok, tok)
+        at = pl.multiple_of(base + (2 * i + 1) * tok, tok)
         ins.append(pltpu.make_async_copy(og_hbm.at[pl.ds(at, tok)], og.at[i], sems.at[i]))
     weights = [
         pltpu.make_async_copy(w_hbm, lhs.at[pl.ds(0, chans)], wsem.at[0]),
@@ -111,7 +144,7 @@
 
 
 def norm_kernel(
-    core_ref, conv_ref, mine_ref, other_ref, got_ref, gain_ref,
+    core_ref, conv_ref, mine_a, other_a, mine_b, other_b, got_ref, gain_ref,
     sw_ref, ng_ref, pay_ref, stat_ref, gg_ref, gcol, gacc, rows,
 ):
     step = pl.program_id(0)
@@ -143,6 +176,9 @@
     for j in range(conv_ref.shape[1] // LANES):
         at = j * LANES
         row = seq * (conv_ref.shape[1] // LANES) + j
+        late = at >= mine_a.shape[1]
+        mine_ref, other_ref = (mine_b, other_b) if late else (mine_a, other_a)
+        near = at - mine_a.shape[1] if late else at
         mean = stat_ref[pl.ds(row, 1)]
         inverse = stat_ref[pl.ds(half + row, 1)]
         s1 = jnp.zeros((8, LANES), F32)
@@ -155,8 +191,8 @@
             sw_ref[c : c + chunk, at : at + LANES] = (scaled * sig).astype(BF16)
             swg = jnp.where(
                 is_mine,
-                mine_ref[c : c + chunk, at : at + LANES],
-                other_ref[c : c + chunk, at : at + LANES].astype(F32),
+                mine_ref[c : c + chunk, near : near + LANES],
+                other_ref[c : c + chunk, near : near + LANES].astype(F32),
             )
             sg = swg * sig * (1.0 + scaled * (1.0 - sig))
             gacc[c : c + chunk] += sg * normed
@@ -176,45 +212,51 @@
             pay_ref[peer] = rows[...]
 
 
-def weight_kernel(
-    core_ref, sw_hbm, sw2_hbm, og_hbm, mine_hbm, other_hbm, lhs, og, mine, other, wsem, sems, osems
-):
+def weight_kernel(sw_ref, og_hbm, out_hbm, og, out, sems, osems):
     n, _, cols = og.shape
-    chans = lhs.shape[0] // 2
-    base = core_ref[0] * (n * cols)
-    ins = []
-    for i in range(n):
-        at = pl.multiple_of(base + i * cols, cols)
-        ins.append(pltpu.make_async_copy(og_hbm.at[:, pl.ds(at, cols)], og.at[i], sems.at[i]))
-    sides = [
-        pltpu.make_async_copy(sw_hbm, lhs.at[pl.ds(0, chans)], wsem.at[0]),
-        pltpu.make_async_copy(sw2_hbm, lhs.at[pl.ds(chans, chans)], wsem.at[1]),
+    ins = [
+        pltpu.make_async_copy(og_hbm.at[:, pl.ds(i * cols, cols)], og.at[i], sems.at[i])
+        for i in range(n)
     ]
-    for c in sides + ins:
+    outs = [
+        pltpu.make_async_copy(out.at[i], out_hbm.at[:, :, pl.ds(i * cols, cols)], osems.at[i])
+        for i in range(n)
+    ]
+    for c in ins:
         c.start()
-    for c in sides:
-        c.wait()
-    outs = []
     for i in range(n):
         ins[i].wait()
-        part = jnp.dot(lhs[...], og[i], preferred_element_type=F32).astype(BF16)
-        mine[i] = part[:chans].reshape(mine.shape[1:])
-        other[i] = part[chans:].reshape(other.shape[1:])
-        here = pl.ds(i * cols, cols)
-        outs += [
-            pltpu.make_async_copy(mine.at[i], mine_hbm.at[:, :, here], osems.at[2 * i]),
-            pltpu.make_async_copy(other.at[i], other_hbm.at[:, :, here], osems.at[2 * i + 1]),
-        ]
-        for c in outs[-2:]:
-            c.start()
+        part = jnp.dot(sw_ref[...], og[i], preferred_element_type=F32)
+        out[i] = part.astype(BF16).reshape(out.shape[1:])
+        outs[i].start()
     for c in outs:
         c.wait()
 
 
-def turn_kernel(
-    blocks, conv_ref, ng_ref, stat_ref, got_ref, cg_ref, head_ref, bias_ref, bias_acc, means
+def grad_kernel(
+    blocks, conv_ref, ng_ref, stat_ref, got_ref, gated_ref, gg_ref, sw_ref, og_hbm, pay_in,
+    cg_ref, head_ref, pay_ref,
+    wide, taps_acc, bias_acc, means, small, og, out, sem, sems, osems,
 ):
     seq = pl.program_id(0)
+    n, _, cols = og.shape
+
+    def fetch(i):
+        at = pl.multiple_of((n + i) * cols, LANES)
+        return pltpu.make_async_copy(og_hbm.at[:, pl.ds(at, cols)], og.at[i], sems.at[i])
+
+    def send(i):
+        at = pl.multiple_of((n + i) * cols, LANES)
+        return pltpu.make_async_copy(out.at[i], pay_ref.at[:, :, pl.ds(at, cols)], osems.at[i])
+
+    @pl.when(seq == 0)
+    def _():
+        fetch(0).start()
+
+    @pl.when(seq < n - 1)
+    def _():
+        fetch(seq + 1).start()
+
     half = stat_ref.shape[0] // 2
     peers = got_ref.shape[0]
     total = peers * LANES
@@ -226,9 +268,13 @@
             s = s + got_ref[p]
         means[...] = s * (1.0 / total)
         bias_acc[...] = jnp.zeros_like(bias_acc)
-
-    for b in range(blocks):
-        here = slice(b * LANES, (b + 1) * LANES)
+        taps_acc[...] = jnp.zeros_like(taps_acc)
+
+    wide[...] = gated_ref[0].astype(F32)
+
+    def block(b, carry):
+        at = b * LANES
+        here = pl.ds(pl.multiple_of(at, LANES), LANES)
         row = seq * blocks + b
         mean = stat_ref[pl.ds(row, 1)]
         inverse = stat_ref[pl.ds(half + row, 1)]
@@ -242,38 +288,6 @@
         for r in range(8, LANES, 8):
             part = part + cg[r : r + 8]
         bias_acc[...] += part
-        if b == 0:
-            head_ref[0] = cg[:PAD]
-
-    @pl.when(seq == pl.num_programs(0) - 1)
-    def _():
-        bias_ref[...] = jnp.sum(bias_acc[...], axis=0, keepdims=True)
-
-
-def taps_kernel(
-    blocks, cg_ref, gated_ref, gg_ref, bias_ref, got_hbm, pay_in,
-    pay_ref, wide, taps_acc, small, came, sem, csems,
-):
-    seq = pl.program_id(0)
-    at = came.shape[2]
-    take = pltpu.make_async_copy(got_hbm, came, csems.at[0])
-    put = pltpu.make_async_copy(came, pay_ref.at[:, :, pl.ds(at, at)], csems.at[1])
-
-    @pl.when(seq == 0)
-    def _():
-        take.start()
-        taps_acc[...] = jnp.zeros_like(taps_acc)
-
-    @pl.when(seq == 1)
-    def _():
-        take.wait()
-        put.start()
-
-    wide[...] = gated_ref[0].astype(F32)
-
-    def block(b, carry):
-        at = b * LANES
-        cg = cg_ref[0, pl.ds(pl.multiple_of(at, LANES), LANES), :]
         for shift, taps in taps_by_shift(lambda tap: tap + PAD - REACH):
             piece = wide[pl.ds(at + shift, LANES + taps[-1][1]), :]
             for tap, skip in taps:
@@ -283,23 +297,35 @@
                 taps_acc[tap] = acc
         return carry
 
-    lax.fori_loop(0, blocks, block, 0, unroll=2)
+    lax.fori_loop(0, blocks // 2, block, 0, unroll=2)
+    fetch(seq).wait()
+    out[seq] = (
+        jnp.dot(sw_ref[...], og[seq], preferred_element_type=F32)
+        .astype(BF16)
+        .reshape(out.shape[1:])
+    )
+    for b in range(blocks // 2, blocks // 2 + 2):
+        block(b, 0)
+    lax.fori_loop(blocks // 2 + 2, blocks, block, 0, unroll=2)
+    send(seq).start()
+    head_ref[0] = cg_ref[0, :PAD]
 
     @pl.when(seq == pl.num_programs(0) - 1)
     def _():
         rows = [jnp.sum(taps_acc[tap], axis=0, keepdims=True) for tap in range(K)]
-        rows += [gg_ref[...], bias_ref[...]]
+        rows += [gg_ref[...], jnp.sum(bias_acc[...], axis=0, keepdims=True)]
         rows += [jnp.zeros((1, LANES), F32)] * (-len(rows) % 8)
         for t in range(len(rows) // 8):
             tile = jnp.concatenate(rows[8 * t : 8 * t + 8], axis=0).astype(BF16)
             for peer in range(small.shape[0]):
                 small[peer, :, t * LANES : (t + 1) * LANES] = tile
         copy = pltpu.make_async_copy(
-            small, pay_ref.at[:, :, pl.ds(2 * at, small.shape[2])], sem
+            small, pay_ref.at[:, :, pl.ds(2 * n * cols, small.shape[2])], sem
         )
         copy.start()
         copy.wait()
-        put.wait()
+        for i in range(n):
+            send(i).wait()
 
 
 def spread_kernel(blocks, cg_ref, next_ref, v_ref, g_ref, taps_ref, vg_ref, gg_ref, wide, tapf):
@@ -330,15 +356,12 @@
     lax.fori_loop(0, blocks, block, 0, unroll=4)
 
 
-def final_kernel(core_ref, got_ref, w_ref, taps_ref, gain_ref, bias_ref):
+def final_kernel(got_ref, w_ref, taps_ref, gain_ref, bias_ref):
     acc = got_ref[0].astype(F32)
     for p in range(1, got_ref.shape[0]):
         acc = acc + got_ref[p].astype(F32)
     width = w_ref.shape[1]
-    half = width // 2
-    for side in range(2):
-        at = pl.multiple_of((core_ref[0] + side) % 2 * half, half)
-        w_ref[:, pl.ds(at, half)] = acc[:, side * half : (side + 1) * half]
+    w_ref[...] = acc[:, :width]
     for t in range(K // 8 + 1):
         tile = acc[:, width + t * LANES : width + (t + 1) * LANES]
         taps_ref[8 * t : min(8 * t + 8, K)] = tile[: min(8, K - 8 * t)]
@@ -351,7 +374,7 @@
     return pl.BlockSpec(shape, lambda i: (0,) * len(shape))
 
 
-PARAMS = pltpu.CompilerParams(vmem_limit_bytes=67_000_000)
+PARAMS = pltpu.CompilerParams(vmem_limit_bytes=67_043_328)
 
 
 def cost(flops, moved):
@@ -381,56 +404,76 @@
     head_block = pl.BlockSpec((1, PAD, chans), lambda i: (i, 0, 0))
     gated_block = pl.BlockSpec((1, length + PAD, chans), lambda i: (i, 0, 0))
     col = pl.BlockSpec((chans, length), lambda i: (0, i))
+    quarter = pl.BlockSpec((chans, length // 4), lambda i: (0, i))
     stats = whole((tp, stat_rows, LANES))
 
     tail = slice(length - PAD, length)
     edge = values_in[:, tail].astype(F32) * sigmoid(gates_in[:, tail].astype(F32))
     halo = lax.ppermute(edge.astype(BF16), "sp", ahead)
     weight2 = lax.ppermute(out_weight, "tp", swap)
-    conv, pay, gated = pl.pallas_call(
+    conv, pay, gated, mine_a, other_a = pl.pallas_call(
         functools.partial(conv_kernel, blocks),
         grid=(seqs,),
-        in_specs=[seq_block, seq_block, head_block, whole((K, chans)), whole((1, chans))],
-        out_specs=[col, stats, gated_block],
+        in_specs=[
+            smem,
+            seq_block,
+            seq_block,
+            head_block,
+            whole((K, chans)),
+            whole((1, chans)),
+            any_,
+            any_,
+            any_,
+        ],
+        out_specs=[col, stats, gated_block, quarter, quarter],
         out_shape=[
             SDS((chans, tokens), F32),
             SDS((tp, stat_rows, LANES), F32),
             SDS((seqs, length + PAD, chans), BF16),
+            SDS((chans, tokens // 4), F32),
+            SDS((chans, tokens // 4), BF16),
         ],
         scratch_shapes=[
             pltpu.VMEM((length + 2 * PAD, chans), F32),
             pltpu.VMEM((PAD, chans), F32),
             pltpu.VMEM((stat_rows, LANES), F32),
+            pltpu.VMEM((2 * chans, width), BF16),
+            pltpu.VMEM((seqs, length // 4, width), BF16),
+            pltpu.SemaphoreType.DMA((2,)),
+            pltpu.SemaphoreType.DMA((seqs,)),
         ],
         compiler_params=PARAMS,
         cost_estimate=cost(2 * K * tokens * chans, 8 << 20),
         name="conv",
-    )(values_in, gates_in, halo, conv_taps, bias_row)
+    )(core, values_in, gates_in, halo, conv_taps, bias_row, out_weight, weight2, flat)
     got = lax.all_to_all(pay, "tp", 0, 0, tiled=True)
 
     pieces = 4
-    mine, other = pl.pallas_call(
+    half = seqs // 2
+    other_a = lax.ppermute(other_a, "tp", swap)
+    mine_b, other_b = pl.pallas_call(
         swish_kernel,
         in_specs=[smem, any_, any_, any_, any_],
         out_specs=[any_, any_],
-        out_shape=[SDS((chans, tokens // 2), F32), SDS((chans, tokens // 2), BF16)],
+        out_shape=[SDS((chans, tokens // 4), F32), SDS((chans, tokens // 4), BF16)],
         scratch_shapes=[
             pltpu.VMEM((2 * chans, width), BF16),
-            pltpu.VMEM((pieces, tokens // 2 // pieces, width), BF16),
-            pltpu.VMEM((chans, tokens // 2), F32),
-            pltpu.VMEM((chans, tokens // 2), BF16),
+            pltpu.VMEM((half, length // 2, width), BF16),
+            pltpu.VMEM((chans, tokens // 4), F32),
+            pltpu.VMEM((chans, tokens // 4), BF16),
             pltpu.SemaphoreType.DMA((2,)),
-            pltpu.SemaphoreType.DMA((pieces,)),
-            pltpu.SemaphoreType.DMA((2 * pieces,)),
+            pltpu.SemaphoreType.DMA((half,)),
+            pltpu.SemaphoreType.DMA((2 * half,)),
         ],
         compiler_params=PARAMS,
-        cost_estimate=cost(2 * tokens * chans * width, tokens * width),
+        cost_estimate=cost(tokens * chans * width, tokens * width // 2),
         name="swish_grad",
     )(core, out_weight, weight2, flat, pay)
-    other = lax.ppermute(other, "tp", swap)
-
-    half = seqs // 2
+    other_b = lax.ppermute(other_b, "tp", swap)
+
     turned = pl.BlockSpec((chans, length), lambda i, c: (0, (i + c[0] * half) % seqs))
+    near = pl.BlockSpec((chans, length // 2), lambda i, c: (0, jnp.minimum(i, half - 1)))
+    far = pl.BlockSpec((chans, length // 2), lambda i, c: (0, jnp.maximum(i, half) - half))
     swished, ng, pay2, stat, gg = pl.pallas_call(
         norm_kernel,
         grid_spec=pltpu.PrefetchScalarGridSpec(
@@ -438,8 +481,10 @@
             grid=(seqs,),
             in_specs=[
                 turned,
-                pl.BlockSpec((chans, length), lambda i, c: (0, jnp.minimum(i, half - 1))),
-                pl.BlockSpec((chans, length), lambda i, c: (0, jnp.maximum(i, half) - half)),
+                near,
+                far,
+                near,
+                far,
                 pl.BlockSpec((tp, stat_rows, LANES), lambda i, c: (0, 0, 0)),
                 pl.BlockSpec((1, chans), lambda i, c: (0, 0)),
             ],
@@ -466,69 +511,69 @@
         compiler_params=PARAMS,
         cost_estimate=cost(30 * tokens * chans, 8 << 20),
         name="norm",
-    )(core, conv, mine, other, got, gain_row)
-    swished2 = lax.ppermute(swished, "tp", swap)
+    )(core, conv, mine_a, other_a, mine_b, other_b, got, gain_row)
     got2 = lax.all_to_all(pay2, "tp", 0, 0, tiled=True)
 
     extra = -(-(K + 2) // 8) * LANES
+    rows = chans // sp
+    pieces = seqs
     cols = width // 2 // pieces
-    part = (sp, chans // sp, width // 2)
-    pay3, other_w = pl.pallas_call(
+    slabs = [
+        pltpu.VMEM((pieces, tokens, cols), BF16),
+        pltpu.VMEM((pieces, sp, rows, cols), BF16),
+    ]
+    pay3 = pl.pallas_call(
         weight_kernel,
-        in_specs=[smem, any_, any_, any_],
-        out_specs=[any_, any_],
-        out_shape=[SDS((sp, chans // sp, width + extra), BF16), SDS(part, BF16)],
+        in_specs=[vmem, any_],
+        out_specs=any_,
+        out_shape=SDS((sp, rows, width + extra), BF16),
         scratch_shapes=[
-            pltpu.VMEM((2 * chans, tokens), BF16),
-            pltpu.VMEM((pieces, tokens, cols), BF16),
-            pltpu.VMEM((pieces, sp, chans // sp, cols), BF16),
-            pltpu.VMEM((pieces, sp, chans // sp, cols), BF16),
-            pltpu.SemaphoreType.DMA((2,)),
+            *slabs,
             pltpu.SemaphoreType.DMA((pieces,)),
-            pltpu.SemaphoreType.DMA((2 * pieces,)),
+            pltpu.SemaphoreType.DMA((pieces,)),
         ],
         compiler_params=PARAMS,
-        cost_estimate=cost(2 * tokens * chans * width, tokens * width),
+        cost_estimate=cost(tokens * chans * width, tokens * width),
         name="weight_grad",
-    )(core, swished, swished2, flat)
-    other_w = lax.ppermute(other_w, "tp", swap)
-
-    cg, head, bias_local = pl.pallas_call(
-        functools.partial(turn_kernel, blocks),
+    )(swished, flat)
+
+    cg, head, pay3 = pl.pallas_call(
+        functools.partial(grad_kernel, blocks),
         grid=(seqs,),
-        in_specs=[col, col, whole((stat_rows, LANES)), stats],
-        out_specs=[seq_block, head_block, whole((1, chans))],
+        in_specs=[
+            col,
+            col,
+            whole((stat_rows, LANES)),
+            stats,
+            gated_block,
+            whole((1, chans)),
+            vmem,
+            any_,
+            any_,
+        ],
+        out_specs=[seq_block, head_block, any_],
         out_shape=[
             SDS((seqs, length, chans), F32),
             SDS((seqs, PAD, chans), F32),
-            SDS((1, chans), F32),
-        ],
-        scratch_shapes=[pltpu.VMEM((8, chans), F32), pltpu.VMEM((stat_rows, LANES), F32)],
-        compiler_params=PARAMS,
-        cost_estimate=cost(30 * tokens * chans, 8 << 20),
-        name="conv_grad",
-    )(conv, ng, stat, got2)
-    after = lax.ppermute(head, "sp", back)
-
-    pay3 = pl.pallas_call(
-        functools.partial(taps_kernel, blocks),
-        grid=(seqs,),
-        in_specs=[seq_block, gated_block, whole((1, chans)), whole((1, chans)), any_, any_],
-        out_specs=any_,
-        out_shape=SDS(pay3.shape, BF16),
+            SDS(pay3.shape, BF16),
+        ],
         scratch_shapes=[
             pltpu.VMEM((length + PAD, chans), F32),
             pltpu.VMEM((K, 8, chans), F32),
-            pltpu.VMEM((sp, chans // sp, extra), BF16),
-            pltpu.VMEM(part, BF16),
+            pltpu.VMEM((8, chans), F32),
+            pltpu.VMEM((stat_rows, LANES), F32),
+            pltpu.VMEM((sp, rows, extra), BF16),
+            *slabs,
             pltpu.SemaphoreType.DMA,
-            pltpu.SemaphoreType.DMA((2,)),
-        ],
-        input_output_aliases={5: 0},
+            pltpu.SemaphoreType.DMA((pieces,)),
+            pltpu.SemaphoreType.DMA((pieces,)),
+        ],
+        input_output_aliases={8: 2},
         compiler_params=PARAMS,
         cost_estimate=cost(2 * K * tokens * chans, 8 << 20),
         name="taps_grad",
-    )(cg, gated, gg, bias_local, other_w, pay3)
+    )(conv, ng, stat, got2, gated, gg, swished, flat, pay3)
+    after = lax.ppermute(head, "sp", back)
     got3 = lax.all_to_all(pay3, "sp", 0, 0, tiled=True)
 
     values_grad, gates_grad = pl.pallas_call(
@@ -545,7 +590,7 @@
 
     weight_grad, taps_grad, gain_grad, bias_grad = pl.pallas_call(
         final_kernel,
-        in_specs=[smem, vmem],
+        in_specs=[vmem],
         out_specs=[vmem] * 4,
         out_shape=[
             SDS((chans // sp, width), F32),
@@ -555,7 +600,7 @@
         ],
         compiler_params=PARAMS,
         name="final_sum",
-    )(core, got3)
+    )(got3)
     gain_grad, bias_grad = gain_grad.reshape(chans), bias_grad.reshape(chans)
     return values_grad, gates_grad, taps_grad, gain_grad, bias_grad, weight_grad
 

time: 118 us -> 108 us (0.915)
  blocking collectives: 23.6 us -> 11.9 us
  starting transfers between devices: 14.3 us -> 18.7 us
  waiting for transfers between devices: 19.7 us -> 17.8 us
  Pallas kernels: 57.2 us -> 55.9 us
    all_to_all x1 -> x0, blocking collectives: 11.5 us -> none  [on_device(): got2 = lax.all_to_all(pay2, 'tp', 0, 0, tiled=True)]
    pallas_call x1, Pallas kernels: 11.1 us -> 6.2 us  [on_device(): pl.pallas_call(swish_kernel, in_specs=[smem, any_, any_, any_, any_], out...]
    all_to_all x0 -> x1, starting transfers between devices: none -> 4.05 us  [on_device(): got2 = lax.all_to_all(pay2, 'tp', 0, 0, tiled=True)]
    pallas_call x1, Pallas kernels: 8.3 us -> 12 us  [on_device(): pl.pallas_call(functools.partial(conv_kernel, blocks), grid=(seqs,), in_s...]
    ppermute x3 -> x2, waiting for transfers between devices: 3 us -> 0.01 us  [the longest x1 0.01 us: on_device(): other_a = lax.ppermute(other_a, 'tp', swap)]
    pallas_call x4 -> x3, Pallas kernels: 24.5 us -> 24.5 us  [the longest x1 13.7 us: on_device(): pl.pallas_call(functools.partial(grad_kernel, blocks), grid=(seqs,), in_s...]
  transfers between devices with their start and end apart: 7 -> 7, of which waited for: 3 -> 2; matrix products, arithmetic and copies ran while one was open for 1% -> 1% of each run, Pallas kernels for 18% -> 21%
where the time goes in v2:
time: 108 us; the launch traced here: 106 us
  Pallas kernels  55.9 us (52%)
  starting transfers between devices  18.7 us (17%)
  waiting for transfers between devices  17.8 us (16%)
  blocking collectives  11.9 us (11%)
    ppermute x1, waiting for transfers between devices, on_device(): after = lax.ppermute(head, 'sp', back)  16.2 us
    pallas_call x1, Pallas kernels, on_device(): pl.pallas_call(functools.partial(grad_kernel, blocks), grid=(seqs,), in_s...  13.7 us
    pallas_call x1, Pallas kernels, on_device(): pl.pallas_call(functools.partial(conv_kernel, blocks), grid=(seqs,), in_s...  12 us
    all_to_all x1, blocking collectives, on_device(): got = lax.all_to_all(pay, 'tp', 0, 0, tiled=True)  11.9 us
    all_to_all x1, starting transfers between devices, on_device(): got3 = lax.all_to_all(pay3, 'sp', 0, 0, tiled=True)  8.98 us
    pallas_call x1, Pallas kernels, on_device(): pl.pallas_call(weight_kernel, in_specs=[vmem, any_], out_specs=any_, out_...  8.67 us
    pallas_call x1, Pallas kernels, on_device(): pl.pallas_call(functools.partial(spread_kernel, blocks), grid=(seqs,), in...  7.63 us
    pallas_call x1, Pallas kernels, on_device(): pl.pallas_call(swish_kernel, in_specs=[smem, any_, any_, any_, any_], out...  6.2 us
  transfers between devices with their start and end apart: 7, of which 2 were waited for; matrix products, arithmetic and copies ran while one was open for 1% of the time, Pallas kernels for 21%

profile of v2, /device:TPU:0, one launch (start us, length us, event | category | flops | bytes accessed | tf_op | source)
XLA Modules:
  0.0 106.5 jit_solution(14426469682512047347)
XLA Ops:
  0.6 0.1 collective-permute-start.1
  0.7 0.8 multiply_convert_fusion
  1.5 3.6 %collective-permute-start = (bf16[4,32,128]{2,1,0:T(8,128)(2,1)S(1)}, bf16[4,32,128]{2,1,0:T(8,128)(2,1)S(1)}, u32[]{:S(2)}, u32[]{:S(2)}) collective-permute-start(bf16[4,32,128]{2,1,0:T(8,128)(2,1)S(1)} %multiply_convert_fusion), channel_id=1, source_target_pairs={{0,8},{8,16},{16,24},{24,32},{32,40},{40,48},{48,56},{56,64},{64,7... | collective-permute-start | bytes 98312 | tf_op jit(solution)/shard_map/ppermute | solution.py:412
  5.1 1.6 %collective-permute-done.halo_ref = bf16[4,32,128]{2,1,0:T(8,128)(2,1)S(1)} collective-permute-done((bf16[4,32,128]{2,1,0:T(8,128)(2,1)S(1)}, bf16[4,32,128]{2,1,0:T(8,128)(2,1)S(1)}, u32[]{:S(2)}, u32[]{:S(2)}) %collective-permute-start) | collective-permute-done | bytes 32800 | tf_op jit(solution)/shard_map/ppermute | solution.py:412
  6.7 0.0 copy-start
  6.7 0.6 copy-done
  7.3 0.0 collective-permute-done.1.w2_hbm
  7.3 12.0 %conv.1 = (f32[128,4096]{1,0:T(8,128)}, f32[8,64,128]{2,1,0:T(8,128)}, bf16[4,1056,128]{2,1,0:T(8,128)(2,1)}, f32[128,1024]{1,0:T(8,128)}, bf16[128,1024]{1,0:T(8,128)(2,1)}) custom-call(s32[1]{0:T(128)} %bitcast.core_ref, bf16[4,1024,128]{2,1,0:T(8,128)(2,1)} %v_ref.3, bf16[4,1024,128]{2,1,0:T(8,128)(2,1)} %g_ref.3, bf16[4,32,128]{2,1,0:T(8,128)(2,1)} %copy-done, ...), custom_call_target="tpu_custom_call" | custom-call | flops 32505856 | bytes 8388608 | tf_op jit(solution)/shard_map/conv/pallas_call | solution.py:414
  19.3 0.1 collective-permute-start.2
  19.4 6.2 %swish_grad.1 = (f32[128,1024]{1,0:T(8,128)}, bf16[128,1024]{1,0:T(8,128)(2,1)}) custom-call(s32[1]{0:T(128)} %bitcast.core_ref, bf16[128,4096]{1,0:T(8,128)(2,1)} %w_hbm.3, bf16[128,4096]{1,0:T(8,128)(2,1)} %collective-permute-done.1.w2_hbm, bf16[4096,4096]{1,0:T(8,128)(2,1)} %bitcast.7, f32[8,64,128]{2,1,0:T(8,128)} %get-tuple-element.30.after_ref), custom_call_target="tpu_custom_call" | custom-call | flops 2147483648 | bytes 8388608 | tf_op jit(solution)/shard_map/swish_grad/pallas_call | solution.py:454
  25.6 0.6 collective-permute-start.3
  26.2 11.9 %all_to_all.15.got_ref = f32[8,64,128]{2,1,0:T(8,128)} all-to-all(f32[8,64,128]{2,1,0:T(8,128)} %get-tuple-element.30.after_ref), channel_id=1, replica_groups=mesh['sp'=16,'tp'=8] {'tp'}, dimensions={0} | all-to-all | bytes 524288 | tf_op jit(solution)/shard_map/all_to_all | solution.py:449
  38.1 0.0 collective-permute-done.2.other_a
  38.1 0.0 collective-permute-done.3.other_b
  38.1 5.7 %norm.1 = (bf16[128,4096]{1,0:T(8,128)(2,1)}, f32[128,4096]{1,0:T(8,128)}, f32[8,64,128]{2,1,0:T(8,128)}, f32[64,128]{1,0:T(8,128)}, f32[1,128]{1,0:T(1,128)}) custom-call(s32[1]{0:T(128)} %bitcast.core_ref, f32[128,4096]{1,0:T(8,128)} %get-tuple-element.27.conv_ref, f32[128,1024]{1,0:T(8,128)} %get-tuple-element.28.mine_a, ...), custom_call_target="tpu_custom_call" | custom-call | flops 15728640 | bytes 8388608 | tf_op jit(solution)/shard_map/norm/pallas_call | solution.py:477
  43.8 4.0 %all-to-all-start.1 = ((f32[8,64,128]{2,1,0:T(8,128)}), f32[8,64,128]{2,1,0:T(8,128)}, u32[]{:S(2)}, u32[]{:S(2)}) async-start(f32[8,64,128]{2,1,0:T(8,128)} %get-tuple-element.35), calls=%async_computation.1 | async-start | bytes 524288 | tf_op jit(solution)/shard_map/all_to_all | solution.py:515
  47.8 8.7 %weight_grad.1.pay_in = bf16[16,8,4736]{2,1,0:T(8,128)(2,1)} custom-call(bf16[128,4096]{1,0:T(8,128)(2,1)} %get-tuple-element.38.sw_ref, bf16[4096,4096]{1,0:T(8,128)(2,1)} %bitcast.8), custom_call_target="tpu_custom_call" | custom-call | flops 2147483648 | bytes 16777216 | tf_op jit(solution)/shard_map/weight_grad/pallas_call | solution.py:525
  56.5 0.0 all-to-all-done.1.got_ref
  56.5 13.7 %taps_grad.1 = (f32[4,1024,128]{2,1,0:T(8,128)}, f32[4,32,128]{2,1,0:T(8,128)}, bf16[16,8,4736]{2,1,0:T(8,128)(2,1)}) custom-call(f32[128,4096]{1,0:T(8,128)} %get-tuple-element.27.conv_ref, f32[128,4096]{1,0:T(8,128)} %get-tuple-element.33.ng_ref, f32[64,128]{1,0:T(8,128)} %get-tuple-element.34.stat_ref, ...), custom_call_target="tpu_custom_call", output_to_operand_aliasing={{2}: (8, {})} | custom-call | flops 32505856 | bytes 8388608 | tf_op jit(solution)/shard_map/taps_grad/pallas_call | solution.py:540
  70.2 0.0 copy-start.1
  70.2 9.0 %all-to-all-start.2 = ((bf16[16,8,4736]{2,1,0:T(8,128)(2,1)}), bf16[16,8,4736]{2,1,0:T(8,128)(2,1)}, u32[]{:S(2)}, u32[]{:S(2)}) async-start(bf16[16,8,4736]{2,1,0:T(8,128)(2,1)} %get-tuple-element.43), calls=%async_computation.2 | async-start | bytes 2424832 | tf_op jit(solution)/shard_map/all_to_all | solution.py:577
  79.2 0.0 copy-done.1
  79.2 1.3 %collective-permute-start.4 = (f32[4,32,128]{2,1,0:T(8,128)S(1)}, f32[4,32,128]{2,1,0:T(8,128)}, u32[]{:S(2)}, u32[]{:S(2)}) collective-permute-start(f32[4,32,128]{2,1,0:T(8,128)S(1)} %copy-done.1), channel_id=1, source_target_pairs={{8,0},{16,8},{24,16},{32,24},{40,32},{48,40},{56,48},{64,56},{72,6... | collective-permute-start | bytes 196616 | tf_op jit(solution)/shard_map/ppermute | solution.py:576
  80.5 16.2 %collective-permute-done.4.next_ref = f32[4,32,128]{2,1,0:T(8,128)} collective-permute-done((f32[4,32,128]{2,1,0:T(8,128)S(1)}, f32[4,32,128]{2,1,0:T(8,128)}, u32[]{:S(2)}, u32[]{:S(2)}) %collective-permute-start.4) | collective-permute-done | bytes 65568 | tf_op jit(solution)/shard_map/ppermute | solution.py:576
  96.7 7.6 %gated_grad.1 = (bf16[4,1024,128]{2,1,0:T(8,128)(2,1)}, bf16[4,1024,128]{2,1,0:T(8,128)(2,1)}) custom-call(f32[4,1024,128]{2,1,0:T(8,128)} %get-tuple-element.39.cg_ref, f32[4,32,128]{2,1,0:T(8,128)} %collective-permute-done.4.next_ref, bf16[4,1024,128]{2,1,0:T(8,128)(2,1)} %v_ref.3, bf16[4,1024,128]{2,1,0:T(8,128)(2,1)} %g_ref.3, bf16[31,128]{1,0:T(8,128)(2,1)} %taps_ref.3), custom_call_target="tpu_custom_call" | custom-call | flops 32505856 | bytes 8388608 | tf_op jit(solution)/shard_map/gated_grad/pallas_call | solution.py:579
  104.4 0.0 all-to-all-done.2.got_ref
  104.4 2.1 %final_sum.1 = (f32[8,4096]{1,0:T(8,128)}, f32[31,128]{1,0:T(8,128)}, f32[1,128]{1,0:T(1,128)}, f32[1,128]{1,0:T(1,128)}) custom-call(bf16[16,8,4736]{2,1,0:T(8,128)(2,1)} %all-to-all-done.2.got_ref), custom_call_target="tpu_custom_call" | custom-call | tf_op jit(solution)/shard_map/final_sum/pallas_call | solution.py:591
Async XLA Ops:
  0.6 6.7 %collective-permute-start.1 = (bf16[128,4096]{1,0:T(8,128)(2,1)}, bf16[128,4096]{1,0:T(8,128)(2,1)}, u32[]{:S(2)}, u32[]{:S(2)}) collective-permute-start(bf16[128,4096]{1,0:T(8,128)(2,1)} %w_hbm.3), channel_id=1, source_target_pairs={{0,1},{1,0},{2,3},{3,2},{4,5},{5,4},{6,7},{7,6},{8,9},{9,8},{10,11... | collective-permute-start | bytes 3145736 | tf_op jit(solution)/shard_map/ppermute | solution.py:413
  1.5 5.2 %collective-permute-start = (bf16[4,32,128]{2,1,0:T(8,128)(2,1)S(1)}, bf16[4,32,128]{2,1,0:T(8,128)(2,1)S(1)}, u32[]{:S(2)}, u32[]{:S(2)}) collective-permute-start(bf16[4,32,128]{2,1,0:T(8,128)(2,1)S(1)} %multiply_convert_fusion), channel_id=1, source_target_pairs={{0,8},{8,16},{16,24},{24,32},{32,40},{40,48},{48,56},{56,64},{64,7... | collective-permute-start | bytes 98312 | tf_op jit(solution)/shard_map/ppermute | solution.py:412
  6.7 0.6 copy-start
  19.3 18.8 %collective-permute-start.2 = (bf16[128,1024]{1,0:T(8,128)(2,1)}, bf16[128,1024]{1,0:T(8,128)(2,1)}, u32[]{:S(2)}, u32[]{:S(2)}) collective-permute-start(bf16[128,1024]{1,0:T(8,128)(2,1)} %get-tuple-element.29), channel_id=1, source_target_pairs={{0,1},{1,0},{2,3},{3,2},{4,5},{5,4},{6,7},{7,6},{8,9},{9,8},{10,11... | collective-permute-start | bytes 786440 | tf_op jit(solution)/shard_map/ppermute | solution.py:453
  25.6 12.5 %collective-permute-start.3 = (bf16[128,1024]{1,0:T(8,128)(2,1)}, bf16[128,1024]{1,0:T(8,128)(2,1)}, u32[]{:S(2)}, u32[]{:S(2)}) collective-permute-start(bf16[128,1024]{1,0:T(8,128)(2,1)} %get-tuple-element.32), channel_id=1, source_target_pairs={{0,1},{1,0},{2,3},{3,2},{4,5},{5,4},{6,7},{7,6},{8,9},{9,8},{10,11... | collective-permute-start | bytes 786440 | tf_op jit(solution)/shard_map/ppermute | solution.py:472
  43.8 12.7 %all-to-all-start.1 = ((f32[8,64,128]{2,1,0:T(8,128)}), f32[8,64,128]{2,1,0:T(8,128)}, u32[]{:S(2)}, u32[]{:S(2)}) async-start(f32[8,64,128]{2,1,0:T(8,128)} %get-tuple-element.35), calls=%async_computation.1 | async-start | bytes 524288 | tf_op jit(solution)/shard_map/all_to_all | solution.py:515
  70.2 9.0 %copy-start.1 = (f32[4,32,128]{2,1,0:T(8,128)S(1)}, f32[4,32,128]{2,1,0:T(8,128)}, u32[]{:S(2)}) copy-start(f32[4,32,128]{2,1,0:T(8,128)} %get-tuple-element.40) | copy-start | bytes 196612
  70.2 34.1 %all-to-all-start.2 = ((bf16[16,8,4736]{2,1,0:T(8,128)(2,1)}), bf16[16,8,4736]{2,1,0:T(8,128)(2,1)}, u32[]{:S(2)}, u32[]{:S(2)}) async-start(bf16[16,8,4736]{2,1,0:T(8,128)(2,1)} %get-tuple-element.43), calls=%async_computation.2 | async-start | bytes 2424832 | tf_op jit(solution)/shard_map/all_to_all | solution.py:577
  79.2 17.5 %collective-permute-start.4 = (f32[4,32,128]{2,1,0:T(8,128)S(1)}, f32[4,32,128]{2,1,0:T(8,128)}, u32[]{:S(2)}, u32[]{:S(2)}) collective-permute-start(f32[4,32,128]{2,1,0:T(8,128)S(1)} %copy-done.1), channel_id=1, source_target_pairs={{8,0},{16,8},{24,16},{32,24},{40,32},{48,40},{56,48},{64,56},{72,6... | collective-permute-start | bytes 196616 | tf_op jit(solution)/shard_map/ppermute | solution.py:576

commit v3 on v2

--- a/solution.py
+++ b/solution.py
@@ -30,7 +30,8 @@
 
 def conv_kernel(
     blocks, core_ref, v_ref, g_ref, halo_ref, taps_ref, bias_ref, w_hbm, w2_hbm, og_hbm,
-    conv_ref, pay_ref, gated_ref, mine_ref, other_ref, wide, tapf, rows, lhs, og, wsem, sems,
+    conv_ref, pay_ref, gated_ref, mine_ref, other_ref,
+    wide, tapf, rows, lhs, og, prod, wsem, sems,
 ):
     seq = pl.program_id(0)
     n, tok, _ = og.shape
@@ -93,11 +94,16 @@
             c.wait()
 
     fetch(seq).wait()
-    out = lax.dot_general(lhs[...], og[seq], (((1,), (1,)), ((), ())), preferred_element_type=F32)
-    mine_ref[...] = out[:chans]
-    other_ref[...] = out[chans:].astype(BF16)
-    for b in range(blocks // 2, blocks):
-        block(b, 0)
+    step = lhs.shape[1] // (blocks // 2)
+    for j in range(blocks // 2):
+        k = slice(j * step, (j + 1) * step)
+        part = lax.dot_general(
+            lhs[:, k], og[seq, :, k], (((1,), (1,)), ((), ())), preferred_element_type=F32
+        )
+        block(blocks // 2 + j, 0)
+        prod[...] = part if j == 0 else prod[...] + part
+    mine_ref[...] = prod[:chans]
+    other_ref[...] = prod[chans:].astype(BF16)
 
     @pl.when(seq == pl.num_programs(0) - 1)
     def _():
@@ -439,6 +445,7 @@
             pltpu.VMEM((stat_rows, LANES), F32),
             pltpu.VMEM((2 * chans, width), BF16),
             pltpu.VMEM((seqs, length // 4, width), BF16),
+            pltpu.VMEM((2 * chans, length // 4), F32),
             pltpu.SemaphoreType.DMA((2,)),
             pltpu.SemaphoreType.DMA((seqs,)),
         ],

time: 108 us -> 108 us (level)
  no operation moved by 1% of the time
where the time goes in v3:
time: 108 us; the launch traced here: 106 us
  Pallas kernels  56 us (52%)
  starting transfers between devices  18.7 us (17%)
  waiting for transfers between devices  17.8 us (16%)
  blocking collectives  11.9 us (11%)
    ppermute x1, waiting for transfers between devices, on_device(): after = lax.ppermute(head, 'sp', back)  16.2 us
    pallas_call x1, Pallas kernels, on_device(): pl.pallas_call(functools.partial(grad_kernel, blocks), grid=(seqs,), in_s...  13.7 us
    pallas_call x1, Pallas kernels, on_device(): pl.pallas_call(functools.partial(conv_kernel, blocks), grid=(seqs,), in_s...  12 us
    all_to_all x1, blocking collectives, on_device(): got = lax.all_to_all(pay, 'tp', 0, 0, tiled=True)  11.9 us
    all_to_all x1, starting transfers between devices, on_device(): got3 = lax.all_to_all(pay3, 'sp', 0, 0, tiled=True)  8.98 us
    pallas_call x1, Pallas kernels, on_device(): pl.pallas_call(weight_kernel, in_specs=[vmem, any_], out_specs=any_, out_...  8.67 us
    pallas_call x1, Pallas kernels, on_device(): pl.pallas_call(functools.partial(spread_kernel, blocks), grid=(seqs,), in...  7.63 us
    pallas_call x1, Pallas kernels, on_device(): pl.pallas_call(swish_kernel, in_specs=[smem, any_, any_, any_, any_], out...  6.2 us
  transfers between devices with their start and end apart: 7, of which 2 were waited for; matrix products, arithmetic and copies ran while one was open for 1% of the time, Pallas kernels for 21%

profile of v3, /device:TPU:0, one launch (start us, length us, event | category | flops | bytes accessed | tf_op | source)
XLA Modules:
  0.0 106.5 jit_solution(3882590735750937340)
XLA Ops:
  0.6 0.1 collective-permute-start.1
  0.7 0.8 multiply_convert_fusion
  1.5 3.6 %collective-permute-start = (bf16[4,32,128]{2,1,0:T(8,128)(2,1)S(1)}, bf16[4,32,128]{2,1,0:T(8,128)(2,1)S(1)}, u32[]{:S(2)}, u32[]{:S(2)}) collective-permute-start(bf16[4,32,128]{2,1,0:T(8,128)(2,1)S(1)} %multiply_convert_fusion), channel_id=1, source_target_pairs={{0,8},{8,16},{16,24},{24,32},{32,40},{40,48},{48,56},{56,64},{64,7... | collective-permute-start | bytes 98312 | tf_op jit(solution)/shard_map/ppermute | solution.py:418
  5.1 1.6 %collective-permute-done.halo_ref = bf16[4,32,128]{2,1,0:T(8,128)(2,1)S(1)} collective-permute-done((bf16[4,32,128]{2,1,0:T(8,128)(2,1)S(1)}, bf16[4,32,128]{2,1,0:T(8,128)(2,1)S(1)}, u32[]{:S(2)}, u32[]{:S(2)}) %collective-permute-start) | collective-permute-done | bytes 32800 | tf_op jit(solution)/shard_map/ppermute | solution.py:418
  6.7 0.0 copy-start
  6.7 0.6 copy-done
  7.3 0.0 collective-permute-done.1.w2_hbm
  7.3 12.0 %conv.1 = (f32[128,4096]{1,0:T(8,128)}, f32[8,64,128]{2,1,0:T(8,128)}, bf16[4,1056,128]{2,1,0:T(8,128)(2,1)}, f32[128,1024]{1,0:T(8,128)}, bf16[128,1024]{1,0:T(8,128)(2,1)}) custom-call(s32[1]{0:T(128)} %bitcast.core_ref, bf16[4,1024,128]{2,1,0:T(8,128)(2,1)} %v_ref.3, bf16[4,1024,128]{2,1,0:T(8,128)(2,1)} %g_ref.3, bf16[4,32,128]{2,1,0:T(8,128)(2,1)} %copy-done, ...), custom_call_target="tpu_custom_call" | custom-call | flops 32505856 | bytes 8388608 | tf_op jit(solution)/shard_map/conv/pallas_call | solution.py:420
  19.3 0.1 collective-permute-start.2
  19.4 6.2 %swish_grad.1 = (f32[128,1024]{1,0:T(8,128)}, bf16[128,1024]{1,0:T(8,128)(2,1)}) custom-call(s32[1]{0:T(128)} %bitcast.core_ref, bf16[128,4096]{1,0:T(8,128)(2,1)} %w_hbm.3, bf16[128,4096]{1,0:T(8,128)(2,1)} %collective-permute-done.1.w2_hbm, bf16[4096,4096]{1,0:T(8,128)(2,1)} %bitcast.7, f32[8,64,128]{2,1,0:T(8,128)} %get-tuple-element.30.after_ref), custom_call_target="tpu_custom_call" | custom-call | flops 2147483648 | bytes 8388608 | tf_op jit(solution)/shard_map/swish_grad/pallas_call | solution.py:461
  25.6 0.6 collective-permute-start.3
  26.2 11.9 %all_to_all.15.got_ref = f32[8,64,128]{2,1,0:T(8,128)} all-to-all(f32[8,64,128]{2,1,0:T(8,128)} %get-tuple-element.30.after_ref), channel_id=1, replica_groups=mesh['sp'=16,'tp'=8] {'tp'}, dimensions={0} | all-to-all | bytes 524288 | tf_op jit(solution)/shard_map/all_to_all | solution.py:456
  38.1 0.0 collective-permute-done.2.other_a
  38.1 0.0 collective-permute-done.3.other_b
  38.1 5.7 %norm.1 = (bf16[128,4096]{1,0:T(8,128)(2,1)}, f32[128,4096]{1,0:T(8,128)}, f32[8,64,128]{2,1,0:T(8,128)}, f32[64,128]{1,0:T(8,128)}, f32[1,128]{1,0:T(1,128)}) custom-call(s32[1]{0:T(128)} %bitcast.core_ref, f32[128,4096]{1,0:T(8,128)} %get-tuple-element.27.conv_ref, f32[128,1024]{1,0:T(8,128)} %get-tuple-element.28.mine_a, ...), custom_call_target="tpu_custom_call" | custom-call | flops 15728640 | bytes 8388608 | tf_op jit(solution)/shard_map/norm/pallas_call | solution.py:484
  43.8 4.0 %all-to-all-start.1 = ((f32[8,64,128]{2,1,0:T(8,128)}), f32[8,64,128]{2,1,0:T(8,128)}, u32[]{:S(2)}, u32[]{:S(2)}) async-start(f32[8,64,128]{2,1,0:T(8,128)} %get-tuple-element.35), calls=%async_computation.1 | async-start | bytes 524288 | tf_op jit(solution)/shard_map/all_to_all | solution.py:522
  47.8 8.7 %weight_grad.1.pay_in = bf16[16,8,4736]{2,1,0:T(8,128)(2,1)} custom-call(bf16[128,4096]{1,0:T(8,128)(2,1)} %get-tuple-element.38.sw_ref, bf16[4096,4096]{1,0:T(8,128)(2,1)} %bitcast.8), custom_call_target="tpu_custom_call" | custom-call | flops 2147483648 | bytes 16777216 | tf_op jit(solution)/shard_map/weight_grad/pallas_call | solution.py:532
  56.5 0.0 all-to-all-done.1.got_ref
  56.5 13.7 %taps_grad.1 = (f32[4,1024,128]{2,1,0:T(8,128)}, f32[4,32,128]{2,1,0:T(8,128)}, bf16[16,8,4736]{2,1,0:T(8,128)(2,1)}) custom-call(f32[128,4096]{1,0:T(8,128)} %get-tuple-element.27.conv_ref, f32[128,4096]{1,0:T(8,128)} %get-tuple-element.33.ng_ref, f32[64,128]{1,0:T(8,128)} %get-tuple-element.34.stat_ref, ...), custom_call_target="tpu_custom_call", output_to_operand_aliasing={{2}: (8, {})} | custom-call | flops 32505856 | bytes 8388608 | tf_op jit(solution)/shard_map/taps_grad/pallas_call | solution.py:547
  70.2 0.0 copy-start.1
  70.2 9.0 %all-to-all-start.2 = ((bf16[16,8,4736]{2,1,0:T(8,128)(2,1)}), bf16[16,8,4736]{2,1,0:T(8,128)(2,1)}, u32[]{:S(2)}, u32[]{:S(2)}) async-start(bf16[16,8,4736]{2,1,0:T(8,128)(2,1)} %get-tuple-element.43), calls=%async_computation.2 | async-start | bytes 2424832 | tf_op jit(solution)/shard_map/all_to_all | solution.py:584
  79.2 0.0 copy-done.1
  79.2 1.3 %collective-permute-start.4 = (f32[4,32,128]{2,1,0:T(8,128)S(1)}, f32[4,32,128]{2,1,0:T(8,128)}, u32[]{:S(2)}, u32[]{:S(2)}) collective-permute-start(f32[4,32,128]{2,1,0:T(8,128)S(1)} %copy-done.1), channel_id=1, source_target_pairs={{8,0},{16,8},{24,16},{32,24},{40,32},{48,40},{56,48},{64,56},{72,6... | collective-permute-start | bytes 196616 | tf_op jit(solution)/shard_map/ppermute | solution.py:583
  80.5 16.2 %collective-permute-done.4.next_ref = f32[4,32,128]{2,1,0:T(8,128)} collective-permute-done((f32[4,32,128]{2,1,0:T(8,128)S(1)}, f32[4,32,128]{2,1,0:T(8,128)}, u32[]{:S(2)}, u32[]{:S(2)}) %collective-permute-start.4) | collective-permute-done | bytes 65568 | tf_op jit(solution)/shard_map/ppermute | solution.py:583
  96.7 7.6 %gated_grad.1 = (bf16[4,1024,128]{2,1,0:T(8,128)(2,1)}, bf16[4,1024,128]{2,1,0:T(8,128)(2,1)}) custom-call(f32[4,1024,128]{2,1,0:T(8,128)} %get-tuple-element.39.cg_ref, f32[4,32,128]{2,1,0:T(8,128)} %collective-permute-done.4.next_ref, bf16[4,1024,128]{2,1,0:T(8,128)(2,1)} %v_ref.3, bf16[4,1024,128]{2,1,0:T(8,128)(2,1)} %g_ref.3, bf16[31,128]{1,0:T(8,128)(2,1)} %taps_ref.3), custom_call_target="tpu_custom_call" | custom-call | flops 32505856 | bytes 8388608 | tf_op jit(solution)/shard_map/gated_grad/pallas_call | solution.py:586
  104.4 0.0 all-to-all-done.2.got_ref
  104.4 2.1 %final_sum.1 = (f32[8,4096]{1,0:T(8,128)}, f32[31,128]{1,0:T(8,128)}, f32[1,128]{1,0:T(1,128)}, f32[1,128]{1,0:T(1,128)}) custom-call(bf16[16,8,4736]{2,1,0:T(8,128)(2,1)} %all-to-all-done.2.got_ref), custom_call_target="tpu_custom_call" | custom-call | tf_op jit(solution)/shard_map/final_sum/pallas_call | solution.py:598
Async XLA Ops:
  0.6 6.7 %collective-permute-start.1 = (bf16[128,4096]{1,0:T(8,128)(2,1)}, bf16[128,4096]{1,0:T(8,128)(2,1)}, u32[]{:S(2)}, u32[]{:S(2)}) collective-permute-start(bf16[128,4096]{1,0:T(8,128)(2,1)} %w_hbm.3), channel_id=1, source_target_pairs={{0,1},{1,0},{2,3},{3,2},{4,5},{5,4},{6,7},{7,6},{8,9},{9,8},{10,11... | collective-permute-start | bytes 3145736 | tf_op jit(solution)/shard_map/ppermute | solution.py:419
  1.5 5.2 %collective-permute-start = (bf16[4,32,128]{2,1,0:T(8,128)(2,1)S(1)}, bf16[4,32,128]{2,1,0:T(8,128)(2,1)S(1)}, u32[]{:S(2)}, u32[]{:S(2)}) collective-permute-start(bf16[4,32,128]{2,1,0:T(8,128)(2,1)S(1)} %multiply_convert_fusion), channel_id=1, source_target_pairs={{0,8},{8,16},{16,24},{24,32},{32,40},{40,48},{48,56},{56,64},{64,7... | collective-permute-start | bytes 98312 | tf_op jit(solution)/shard_map/ppermute | solution.py:418
  6.7 0.6 copy-start
  19.3 18.8 %collective-permute-start.2 = (bf16[128,1024]{1,0:T(8,128)(2,1)}, bf16[128,1024]{1,0:T(8,128)(2,1)}, u32[]{:S(2)}, u32[]{:S(2)}) collective-permute-start(bf16[128,1024]{1,0:T(8,128)(2,1)} %get-tuple-element.29), channel_id=1, source_target_pairs={{0,1},{1,0},{2,3},{3,2},{4,5},{5,4},{6,7},{7,6},{8,9},{9,8},{10,11... | collective-permute-start | bytes 786440 | tf_op jit(solution)/shard_map/ppermute | solution.py:460
  25.6 12.5 %collective-permute-start.3 = (bf16[128,1024]{1,0:T(8,128)(2,1)}, bf16[128,1024]{1,0:T(8,128)(2,1)}, u32[]{:S(2)}, u32[]{:S(2)}) collective-permute-start(bf16[128,1024]{1,0:T(8,128)(2,1)} %get-tuple-element.32), channel_id=1, source_target_pairs={{0,1},{1,0},{2,3},{3,2},{4,5},{5,4},{6,7},{7,6},{8,9},{9,8},{10,11... | collective-permute-start | bytes 786440 | tf_op jit(solution)/shard_map/ppermute | solution.py:479
  43.8 12.7 %all-to-all-start.1 = ((f32[8,64,128]{2,1,0:T(8,128)}), f32[8,64,128]{2,1,0:T(8,128)}, u32[]{:S(2)}, u32[]{:S(2)}) async-start(f32[8,64,128]{2,1,0:T(8,128)} %get-tuple-element.35), calls=%async_computation.1 | async-start | bytes 524288 | tf_op jit(solution)/shard_map/all_to_all | solution.py:522
  70.2 9.0 %copy-start.1 = (f32[4,32,128]{2,1,0:T(8,128)S(1)}, f32[4,32,128]{2,1,0:T(8,128)}, u32[]{:S(2)}) copy-start(f32[4,32,128]{2,1,0:T(8,128)} %get-tuple-element.40) | copy-start | bytes 196612
  70.2 34.1 %all-to-all-start.2 = ((bf16[16,8,4736]{2,1,0:T(8,128)(2,1)}), bf16[16,8,4736]{2,1,0:T(8,128)(2,1)}, u32[]{:S(2)}, u32[]{:S(2)}) async-start(bf16[16,8,4736]{2,1,0:T(8,128)(2,1)} %get-tuple-element.43), calls=%async_computation.2 | async-start | bytes 2424832 | tf_op jit(solution)/shard_map/all_to_all | solution.py:584
  79.2 17.5 %collective-permute-start.4 = (f32[4,32,128]{2,1,0:T(8,128)S(1)}, f32[4,32,128]{2,1,0:T(8,128)}, u32[]{:S(2)}, u32[]{:S(2)}) collective-permute-start(f32[4,32,128]{2,1,0:T(8,128)S(1)} %copy-done.1), channel_id=1, source_target_pairs={{8,0},{16,8},{24,16},{32,24},{40,32},{48,40},{56,48},{64,56},{72,6... | collective-permute-start | bytes 196616 | tf_op jit(solution)/shard_map/ppermute | solution.py:583

commit v4 on v2

--- a/solution.py
+++ b/solution.py
@@ -54,10 +54,6 @@
             c.start()
         fetch(0).start()
         tapf[:K] = taps_ref[...].astype(F32)
-
-    @pl.when(seq < n - 1)
-    def _():
-        fetch(seq + 1).start()
 
     gated_ref[0, :PAD] = halo_ref[0]
     wide[:PAD] = halo_ref[0].astype(F32)
@@ -93,6 +89,11 @@
             c.wait()
 
     fetch(seq).wait()
+
+    @pl.when(seq < n - 1)
+    def _():
+        fetch(seq + 1).start()
+
     out = lax.dot_general(lhs[...], og[seq], (((1,), (1,)), ((), ())), preferred_element_type=F32)
     mine_ref[...] = out[:chans]
     other_ref[...] = out[chans:].astype(BF16)
@@ -234,12 +235,13 @@
 
 
 def grad_kernel(
-    blocks, conv_ref, ng_ref, stat_ref, got_ref, gated_ref, gg_ref, sw_ref, og_hbm, pay_in,
+    blocks, conv_ref, ng_ref, stat_ref, got_ref, gated_ref, gg_ref, sw_hbm, og_hbm, pay_in,
     cg_ref, head_ref, pay_ref,
-    wide, taps_acc, bias_acc, means, small, og, out, sem, sems, osems,
+    wide, taps_acc, bias_acc, means, small, og, out, sw_ref, sem, sems, osems,
 ):
     seq = pl.program_id(0)
     n, _, cols = og.shape
+    side = pltpu.make_async_copy(sw_hbm, sw_ref, sem)
 
     def fetch(i):
         at = pl.multiple_of((n + i) * cols, LANES)
@@ -251,11 +253,8 @@
 
     @pl.when(seq == 0)
     def _():
+        side.start()
         fetch(0).start()
-
-    @pl.when(seq < n - 1)
-    def _():
-        fetch(seq + 1).start()
 
     half = stat_ref.shape[0] // 2
     peers = got_ref.shape[0]
@@ -299,6 +298,15 @@
 
     lax.fori_loop(0, blocks // 2, block, 0, unroll=2)
     fetch(seq).wait()
+
+    @pl.when(seq < n - 1)
+    def _():
+        fetch(seq + 1).start()
+
+    @pl.when(seq == 0)
+    def _():
+        side.wait()
+
     out[seq] = (
         jnp.dot(sw_ref[...], og[seq], preferred_element_type=F32)
         .astype(BF16)
@@ -547,7 +555,7 @@
             stats,
             gated_block,
             whole((1, chans)),
-            vmem,
+            any_,
             any_,
             any_,
         ],
@@ -564,6 +572,7 @@
             pltpu.VMEM((stat_rows, LANES), F32),
             pltpu.VMEM((sp, rows, extra), BF16),
             *slabs,
+            pltpu.VMEM((chans, tokens), BF16),
             pltpu.SemaphoreType.DMA,
             pltpu.SemaphoreType.DMA((pieces,)),
             pltpu.SemaphoreType.DMA((pieces,)),

time: 108 us -> 108 us (level)
  no operation moved by 1% of the time
where the time goes in v4:
time: 108 us; the launch traced here: 107 us
  Pallas kernels  56 us (52%)
  starting transfers between devices  18.6 us (17%)
  waiting for transfers between devices  17.8 us (16%)
  blocking collectives  11.9 us (11%)
    ppermute x1, waiting for transfers between devices, on_device(): after = lax.ppermute(head, 'sp', back)  16.2 us
    pallas_call x1, Pallas kernels, on_device(): pl.pallas_call(functools.partial(grad_kernel, blocks), grid=(seqs,), in_s...  13.7 us
    pallas_call x1, Pallas kernels, on_device(): pl.pallas_call(functools.partial(conv_kernel, blocks), grid=(seqs,), in_s...  12 us
    all_to_all x1, blocking collectives, on_device(): got = lax.all_to_all(pay, 'tp', 0, 0, tiled=True)  11.9 us
    all_to_all x1, starting transfers between devices, on_device(): got3 = lax.all_to_all(pay3, 'sp', 0, 0, tiled=True)  8.98 us
    pallas_call x1, Pallas kernels, on_device(): pl.pallas_call(weight_kernel, in_specs=[vmem, any_], out_specs=any_, out_...  8.67 us
    pallas_call x1, Pallas kernels, on_device(): pl.pallas_call(functools.partial(spread_kernel, blocks), grid=(seqs,), in...  7.63 us
    pallas_call x1, Pallas kernels, on_device(): pl.pallas_call(swish_kernel, in_specs=[smem, any_, any_, any_, any_], out...  6.21 us
  transfers between devices with their start and end apart: 7, of which 2 were waited for; matrix products, arithmetic and copies ran while one was open for 1% of the time, Pallas kernels for 21%

profile of v4, /device:TPU:0, one launch (start us, length us, event | category | flops | bytes accessed | tf_op | source)
XLA Modules:
  0.0 106.5 jit_solution(14580399405911767869)
XLA Ops:
  0.6 0.1 collective-permute-start.1
  0.7 0.8 multiply_convert_fusion
  1.5 3.6 %collective-permute-start = (bf16[4,32,128]{2,1,0:T(8,128)(2,1)S(1)}, bf16[4,32,128]{2,1,0:T(8,128)(2,1)S(1)}, u32[]{:S(2)}, u32[]{:S(2)}) collective-permute-start(bf16[4,32,128]{2,1,0:T(8,128)(2,1)S(1)} %multiply_convert_fusion), channel_id=1, source_target_pairs={{0,8},{8,16},{16,24},{24,32},{32,40},{40,48},{48,56},{56,64},{64,7... | collective-permute-start | bytes 98312 | tf_op jit(solution)/shard_map/ppermute | solution.py:420
  5.1 1.6 %collective-permute-done.halo_ref = bf16[4,32,128]{2,1,0:T(8,128)(2,1)S(1)} collective-permute-done((bf16[4,32,128]{2,1,0:T(8,128)(2,1)S(1)}, bf16[4,32,128]{2,1,0:T(8,128)(2,1)S(1)}, u32[]{:S(2)}, u32[]{:S(2)}) %collective-permute-start) | collective-permute-done | bytes 32800 | tf_op jit(solution)/shard_map/ppermute | solution.py:420
  6.7 0.0 copy-start
  6.7 0.6 copy-done
  7.3 0.0 collective-permute-done.1.w2_hbm
  7.3 12.0 %conv.1 = (f32[128,4096]{1,0:T(8,128)}, f32[8,64,128]{2,1,0:T(8,128)}, bf16[4,1056,128]{2,1,0:T(8,128)(2,1)}, f32[128,1024]{1,0:T(8,128)}, bf16[128,1024]{1,0:T(8,128)(2,1)}) custom-call(s32[1]{0:T(128)} %bitcast.core_ref, bf16[4,1024,128]{2,1,0:T(8,128)(2,1)} %v_ref.3, bf16[4,1024,128]{2,1,0:T(8,128)(2,1)} %g_ref.3, bf16[4,32,128]{2,1,0:T(8,128)(2,1)} %copy-done, ...), custom_call_target="tpu_custom_call" | custom-call | flops 32505856 | bytes 8388608 | tf_op jit(solution)/shard_map/conv/pallas_call | solution.py:422
  19.4 0.1 collective-permute-start.2
  19.5 6.2 %swish_grad.1 = (f32[128,1024]{1,0:T(8,128)}, bf16[128,1024]{1,0:T(8,128)(2,1)}) custom-call(s32[1]{0:T(128)} %bitcast.core_ref, bf16[128,4096]{1,0:T(8,128)(2,1)} %w_hbm.3, bf16[128,4096]{1,0:T(8,128)(2,1)} %collective-permute-done.1.w2_hbm, bf16[4096,4096]{1,0:T(8,128)(2,1)} %bitcast.7, f32[8,64,128]{2,1,0:T(8,128)} %get-tuple-element.30.after_ref), custom_call_target="tpu_custom_call" | custom-call | flops 2147483648 | bytes 8388608 | tf_op jit(solution)/shard_map/swish_grad/pallas_call | solution.py:462
  25.7 0.6 collective-permute-start.3
  26.2 11.9 %all_to_all.15.got_ref = f32[8,64,128]{2,1,0:T(8,128)} all-to-all(f32[8,64,128]{2,1,0:T(8,128)} %get-tuple-element.30.after_ref), channel_id=1, replica_groups=mesh['sp'=16,'tp'=8] {'tp'}, dimensions={0} | all-to-all | bytes 524288 | tf_op jit(solution)/shard_map/all_to_all | solution.py:457
  38.1 0.0 collective-permute-done.2.other_a
  38.1 0.0 collective-permute-done.3.other_b
  38.2 5.7 %norm.1 = (bf16[128,4096]{1,0:T(8,128)(2,1)}, f32[128,4096]{1,0:T(8,128)}, f32[8,64,128]{2,1,0:T(8,128)}, f32[64,128]{1,0:T(8,128)}, f32[1,128]{1,0:T(1,128)}) custom-call(s32[1]{0:T(128)} %bitcast.core_ref, f32[128,4096]{1,0:T(8,128)} %get-tuple-element.27.conv_ref, f32[128,1024]{1,0:T(8,128)} %get-tuple-element.28.mine_a, ...), custom_call_target="tpu_custom_call" | custom-call | flops 15728640 | bytes 8388608 | tf_op jit(solution)/shard_map/norm/pallas_call | solution.py:485
  43.8 4.0 %all-to-all-start.1 = ((f32[8,64,128]{2,1,0:T(8,128)}), f32[8,64,128]{2,1,0:T(8,128)}, u32[]{:S(2)}, u32[]{:S(2)}) async-start(f32[8,64,128]{2,1,0:T(8,128)} %get-tuple-element.35), calls=%async_computation.1 | async-start | bytes 524288 | tf_op jit(solution)/shard_map/all_to_all | solution.py:523
  47.9 8.7 %weight_grad.1.pay_in = bf16[16,8,4736]{2,1,0:T(8,128)(2,1)} custom-call(bf16[128,4096]{1,0:T(8,128)(2,1)} %get-tuple-element.38.sw_ref.sw_hbm, bf16[4096,4096]{1,0:T(8,128)(2,1)} %bitcast.8), custom_call_target="tpu_custom_call" | custom-call | flops 2147483648 | bytes 16777216 | tf_op jit(solution)/shard_map/weight_grad/pallas_call | solution.py:533
  56.6 0.0 all-to-all-done.1.got_ref
  56.6 13.7 %taps_grad.1 = (f32[4,1024,128]{2,1,0:T(8,128)}, f32[4,32,128]{2,1,0:T(8,128)}, bf16[16,8,4736]{2,1,0:T(8,128)(2,1)}) custom-call(f32[128,4096]{1,0:T(8,128)} %get-tuple-element.27.conv_ref, f32[128,4096]{1,0:T(8,128)} %get-tuple-element.33.ng_ref, f32[64,128]{1,0:T(8,128)} %get-tuple-element.34.stat_ref, ...), custom_call_target="tpu_custom_call", output_to_operand_aliasing={{2}: (8, {})} | custom-call | flops 32505856 | bytes 8388608 | tf_op jit(solution)/shard_map/taps_grad/pallas_call | solution.py:548
  70.3 0.0 copy-start.1
  70.3 9.0 %all-to-all-start.2 = ((bf16[16,8,4736]{2,1,0:T(8,128)(2,1)}), bf16[16,8,4736]{2,1,0:T(8,128)(2,1)}, u32[]{:S(2)}, u32[]{:S(2)}) async-start(bf16[16,8,4736]{2,1,0:T(8,128)(2,1)} %get-tuple-element.43), calls=%async_computation.2 | async-start | bytes 2424832 | tf_op jit(solution)/shard_map/all_to_all | solution.py:586
  79.3 0.0 copy-done.1
  79.3 1.3 %collective-permute-start.4 = (f32[4,32,128]{2,1,0:T(8,128)S(1)}, f32[4,32,128]{2,1,0:T(8,128)}, u32[]{:S(2)}, u32[]{:S(2)}) collective-permute-start(f32[4,32,128]{2,1,0:T(8,128)S(1)} %copy-done.1), channel_id=1, source_target_pairs={{8,0},{16,8},{24,16},{32,24},{40,32},{48,40},{56,48},{64,56},{72,6... | collective-permute-start | bytes 196616 | tf_op jit(solution)/shard_map/ppermute | solution.py:585
  80.6 16.2 %collective-permute-done.4.next_ref = f32[4,32,128]{2,1,0:T(8,128)} collective-permute-done((f32[4,32,128]{2,1,0:T(8,128)S(1)}, f32[4,32,128]{2,1,0:T(8,128)}, u32[]{:S(2)}, u32[]{:S(2)}) %collective-permute-start.4) | collective-permute-done | bytes 65568 | tf_op jit(solution)/shard_map/ppermute | solution.py:585
  96.8 7.6 %gated_grad.1 = (bf16[4,1024,128]{2,1,0:T(8,128)(2,1)}, bf16[4,1024,128]{2,1,0:T(8,128)(2,1)}) custom-call(f32[4,1024,128]{2,1,0:T(8,128)} %get-tuple-element.39.cg_ref, f32[4,32,128]{2,1,0:T(8,128)} %collective-permute-done.4.next_ref, bf16[4,1024,128]{2,1,0:T(8,128)(2,1)} %v_ref.3, bf16[4,1024,128]{2,1,0:T(8,128)(2,1)} %g_ref.3, bf16[31,128]{1,0:T(8,128)(2,1)} %taps_ref.3), custom_call_target="tpu_custom_call" | custom-call | flops 32505856 | bytes 8388608 | tf_op jit(solution)/shard_map/gated_grad/pallas_call | solution.py:588
  104.4 0.0 all-to-all-done.2.got_ref
  104.4 2.1 %final_sum.1 = (f32[8,4096]{1,0:T(8,128)}, f32[31,128]{1,0:T(8,128)}, f32[1,128]{1,0:T(1,128)}, f32[1,128]{1,0:T(1,128)}) custom-call(bf16[16,8,4736]{2,1,0:T(8,128)(2,1)} %all-to-all-done.2.got_ref), custom_call_target="tpu_custom_call" | custom-call | tf_op jit(solution)/shard_map/final_sum/pallas_call | solution.py:600
Async XLA Ops:
  0.6 6.7 %collective-permute-start.1 = (bf16[128,4096]{1,0:T(8,128)(2,1)}, bf16[128,4096]{1,0:T(8,128)(2,1)}, u32[]{:S(2)}, u32[]{:S(2)}) collective-permute-start(bf16[128,4096]{1,0:T(8,128)(2,1)} %w_hbm.3), channel_id=1, source_target_pairs={{0,1},{1,0},{2,3},{3,2},{4,5},{5,4},{6,7},{7,6},{8,9},{9,8},{10,11... | collective-permute-start | bytes 3145736 | tf_op jit(solution)/shard_map/ppermute | solution.py:421
  1.5 5.2 %collective-permute-start = (bf16[4,32,128]{2,1,0:T(8,128)(2,1)S(1)}, bf16[4,32,128]{2,1,0:T(8,128)(2,1)S(1)}, u32[]{:S(2)}, u32[]{:S(2)}) collective-permute-start(bf16[4,32,128]{2,1,0:T(8,128)(2,1)S(1)} %multiply_convert_fusion), channel_id=1, source_target_pairs={{0,8},{8,16},{16,24},{24,32},{32,40},{40,48},{48,56},{56,64},{64,7... | collective-permute-start | bytes 98312 | tf_op jit(solution)/shard_map/ppermute | solution.py:420
  6.7 0.6 copy-start
  19.4 18.8 %collective-permute-start.2 = (bf16[128,1024]{1,0:T(8,128)(2,1)}, bf16[128,1024]{1,0:T(8,128)(2,1)}, u32[]{:S(2)}, u32[]{:S(2)}) collective-permute-start(bf16[128,1024]{1,0:T(8,128)(2,1)} %get-tuple-element.29), channel_id=1, source_target_pairs={{0,1},{1,0},{2,3},{3,2},{4,5},{5,4},{6,7},{7,6},{8,9},{9,8},{10,11... | collective-permute-start | bytes 786440 | tf_op jit(solution)/shard_map/ppermute | solution.py:461
  25.7 12.5 %collective-permute-start.3 = (bf16[128,1024]{1,0:T(8,128)(2,1)}, bf16[128,1024]{1,0:T(8,128)(2,1)}, u32[]{:S(2)}, u32[]{:S(2)}) collective-permute-start(bf16[128,1024]{1,0:T(8,128)(2,1)} %get-tuple-element.32), channel_id=1, source_target_pairs={{0,1},{1,0},{2,3},{3,2},{4,5},{5,4},{6,7},{7,6},{8,9},{9,8},{10,11... | collective-permute-start | bytes 786440 | tf_op jit(solution)/shard_map/ppermute | solution.py:480
  43.8 12.7 %all-to-all-start.1 = ((f32[8,64,128]{2,1,0:T(8,128)}), f32[8,64,128]{2,1,0:T(8,128)}, u32[]{:S(2)}, u32[]{:S(2)}) async-start(f32[8,64,128]{2,1,0:T(8,128)} %get-tuple-element.35), calls=%async_computation.1 | async-start | bytes 524288 | tf_op jit(solution)/shard_map/all_to_all | solution.py:523
  70.3 9.0 %copy-start.1 = (f32[4,32,128]{2,1,0:T(8,128)S(1)}, f32[4,32,128]{2,1,0:T(8,128)}, u32[]{:S(2)}) copy-start(f32[4,32,128]{2,1,0:T(8,128)} %get-tuple-element.40) | copy-start | bytes 196612
  70.3 34.1 %all-to-all-start.2 = ((bf16[16,8,4736]{2,1,0:T(8,128)(2,1)}), bf16[16,8,4736]{2,1,0:T(8,128)(2,1)}, u32[]{:S(2)}, u32[]{:S(2)}) async-start(bf16[16,8,4736]{2,1,0:T(8,128)(2,1)} %get-tuple-element.43), calls=%async_computation.2 | async-start | bytes 2424832 | tf_op jit(solution)/shard_map/all_to_all | solution.py:586
  79.3 17.5 %collective-permute-start.4 = (f32[4,32,128]{2,1,0:T(8,128)S(1)}, f32[4,32,128]{2,1,0:T(8,128)}, u32[]{:S(2)}, u32[]{:S(2)}) collective-permute-start(f32[4,32,128]{2,1,0:T(8,128)S(1)} %copy-done.1), channel_id=1, source_target_pairs={{8,0},{16,8},{24,16},{32,24},{40,32},{48,40},{56,48},{64,56},{72,6... | collective-permute-start | bytes 196616 | tf_op jit(solution)/shard_map/ppermute | solution.py:585
